TPU v7x, 512 devices: a whole 4x8x8 slice. The times are simulated.
512 devices in a mesh: ep: 32 (over z, x), tp: 16 (over y, core).
Axes of the slice: x: 4, y: 8, z: 8, core: 2. Of those that a mesh axis runs over, the one named last changes fastest.
Arguments:
- mix_input: bfloat16 [16384, 2048], P('ep', 'tp'), may hold values from -6 to 6
- mix_weight: bfloat16 [2048, 4096], P(None, 'tp'), may hold values from -0.125 to 0.125
- expert_input: bfloat16 [4096, 4096], P('ep', 'tp'), may hold values from -4500 to 4500
- expert_index: int32 [4096, 2], P('ep'), may hold values from 0 to 31, as said below
- route_share: float32 [4096, 2], P('ep'), may hold values from 0.1 to 1
- norm_gain: float32 [4096], replicated, may hold values from 0.1 to 1.9
- gate_weight: bfloat16 [32, 4096, 2048], P('ep', None, 'tp'), may hold values from -0.09375 to 0.09375
- up_weight: bfloat16 [32, 4096, 2048], P('ep', None, 'tp'), may hold values from -0.09375 to 0.09375
- down_weight: bfloat16 [32, 2048, 4096], P('ep', None, 'tp'), may hold values from -0.125 to 0.125
Outputs:
- mixed_rows: bfloat16 [16384, 4096], P('ep', 'tp')
- expert_rows: bfloat16 [4096, 4096], P('ep', 'tp')
Inputs may be any that keep to these rules, and one draw needn't show every extreme that they name: `expert_index`: each row names 2 different experts. Within each aligned block of 128 rows (the rows of one index of ep) no expert is named by more than 16 rows, and one expert, the same in every block, is named by exactly 16 rows.
All inputs are finite; a program needn't handle non-finite values.
Results may differ from a plain program's by a relative error of at most 0.007.
Values may be sent and summed in bfloat16 or wider, within the bound.
A program may use at most 64 MiB of HBM per device.

v0:
```python
import jax
import jax.numpy as jnp
from jax import lax
from jax.sharding import PartitionSpec as P

POOL = 2048
TOP = 2


window_reach = 15
norm_eps = 1e-06


def passed_along(value, axis, by):
    size = lax.axis_size(axis)
    pairs = [(i, i + by) for i in range(size) if 0 <= i + by < size]
    return lax.ppermute(value, axis, pairs)


def laid_out(parts, dim):
    lengths = list(parts.shape[1:])
    lengths[dim] *= parts.shape[0]
    return jnp.moveaxis(parts, 0, dim).reshape(lengths)


def copy_for_each(value, axis):
    size = lax.axis_size(axis)
    return lax.all_to_all(
        jnp.broadcast_to(value[None], (size, *value.shape)), axis, 0, 0, tiled=True
    )


def gathered_copies(value, axis, dim):
    return laid_out(copy_for_each(value, axis), dim)


def pool_minus_self(extended, first_pos, group_size, channel_base):
    length = extended.shape[0] - window_reach
    channels = extended.shape[1]
    channel = channel_base + jnp.arange(channels, dtype=jnp.int32)
    window = jnp.power(2, channel // group_size + 1).astype(jnp.int32)
    running = jnp.zeros((length, channels), jnp.float32)
    for lag_count in range(window_reach + 1):
        shifted = extended[window_reach - lag_count : window_reach - lag_count + length]
        running = running + jnp.where(lag_count < window[None, :], shifted, 0.0)
    position = first_pos + jnp.arange(length, dtype=jnp.int32)
    counts = jnp.minimum(position[:, None] + 1, window[None, :]).astype(jnp.float32)
    return (running / counts - extended[window_reach:]).astype(jnp.bfloat16)


def slot_targets(indices, experts, capacity):
    flattened = indices.reshape(-1)
    one_hot = (flattened[:, None] == jnp.arange(experts, dtype=jnp.int32)[None, :]).astype(
        jnp.int32
    )
    earlier = jnp.cumsum(one_hot, axis=0) - one_hot
    return flattened * capacity + jnp.sum(earlier * one_hot, axis=1)


def shards(
    mix_input,
    mix_weight,
    expert_input,
    expert_index,
    route_share,
    norm_gain,
    gate_weight,
    up_weight,
    down_weight,
):
    tokens_mix, channels = mix_input.shape
    trailing = mix_input[tokens_mix - window_reach :]
    previous = passed_along(trailing, "ep", 1)
    extended = jnp.concatenate([previous, mix_input], axis=0).astype(jnp.float32)
    pooled = pool_minus_self(
        extended, lax.axis_index("ep") * tokens_mix, POOL // 4, lax.axis_index("tp") * channels
    )
    mixed_rows = jnp.dot(
        lax.all_gather(pooled, "tp", axis=1, tiled=True),
        mix_weight,
        preferred_element_type=jnp.float32,
    ).astype(jnp.bfloat16)
    tokens_exp = expert_input.shape[0]
    local_experts = gate_weight.shape[0]
    experts = local_experts * lax.axis_size("ep")
    capacity = 2 * tokens_exp * TOP // experts
    model_width = norm_gain.shape[0]
    targets = slot_targets(expert_index, experts, capacity)
    sources = jnp.repeat(jnp.arange(tokens_exp, dtype=jnp.int32), TOP)
    table = jnp.full((experts * capacity,), tokens_exp, jnp.int32).at[targets].set(sources)
    feature_block = expert_input.shape[1]
    padded = jnp.concatenate([expert_input, jnp.zeros((1, feature_block), jnp.bfloat16)], axis=0)
    outgoing = padded[table].reshape(experts, capacity, feature_block)
    arrived = lax.all_to_all(outgoing, "ep", split_axis=0, concat_axis=1, tiled=True)
    portion = lax.all_gather(arrived, "tp", axis=2, tiled=True)
    scaled = (portion.astype(jnp.float32) * norm_gain).astype(jnp.bfloat16)
    gate_acts = jnp.einsum("erd,edh->erh", scaled, gate_weight, preferred_element_type=jnp.float32)
    up_acts = jnp.einsum("erd,edh->erh", scaled, up_weight, preferred_element_type=jnp.float32)
    squares = jnp.sum(jnp.square(portion.astype(jnp.float32)), axis=2)
    inverse = lax.rsqrt(squares / model_width + norm_eps)[:, :, None]
    hidden = (jax.nn.silu(gate_acts * inverse) * (up_acts * inverse)).astype(jnp.bfloat16)
    produced = jnp.einsum(
        "erh,ehc->erc",
        gathered_copies(hidden, "tp", 2),
        down_weight,
        preferred_element_type=jnp.float32,
    ).astype(jnp.bfloat16)
    returned = lax.all_to_all(produced, "ep", split_axis=1, concat_axis=0, tiled=True)
    returned = returned.reshape(experts * capacity, returned.shape[2])
    picked = returned[targets].astype(jnp.float32).reshape(tokens_exp, TOP, returned.shape[1])
    shares = route_share / jnp.sum(route_share, axis=1, keepdims=True)
    expert_rows = jnp.sum(picked * shares[:, :, None], axis=1).astype(jnp.bfloat16)
    return (mixed_rows, expert_rows)


def solution(mesh):
    placed = (
        P("ep", "tp"),
        P(None, "tp"),
        P("ep", "tp"),
        P("ep", None),
        P("ep", None),
        P(),
        P("ep", None, "tp"),
        P("ep", None, "tp"),
        P("ep", None, "tp"),
    )
    return jax.shard_map(
        shards,
        mesh=mesh,
        in_specs=placed,
        out_specs=(P("ep", "tp"), P("ep", "tp")),
        check_vma=False,
    )
```

profile of v0, /device:TPU:1, one launch (start us, length us, event | category | flops | bytes accessed | tf_op | source)
XLA Modules:
  0.0 190.6 jit_solution(15322384750593228259)
XLA Ops:
  7.2 0.8 broadcast_multiply_fusion
  8.1 0.8 copy.27
  9.0 0.1 eq.25
  9.2 0.1 mul.314
  9.4 0.6 reduce-window.6
  10.0 0.2 slice_reduce_fusion
  10.5 1.4 scatter_custom_fusion
  11.9 0.8 concatenate.7
  12.8 1.9 %gather_fusion = bf16[512,256]{1,0:T(8,128)(2,1)S(1)} fusion(bf16[129,256]{1,0:T(8,128)(2,1)S(1)} %concatenate.7, s32[1024]{0:T(1024)S(1)} %pad_clamp_fusion.1), kind=kCustom, calls=%fused_computation | custom fusion | bytes 526336 | tf_op jit(solution)/shard_map/gather | solution.py:93
  14.7 24.9 %all_to_all.26 = bf16[32,16,256]{2,1,0:T(8,128)(2,1)} all-to-all(bf16[32,16,256]{2,1,0:T(8,128)(2,1)S(1)} %bitcast.67), channel_id=1, replica_groups=mesh['ep'=32,'tp'=16] {'ep'}, dimensions={0} | all-to-all | bytes 524288 | tf_op jit(solution)/shard_map/all_to_all | solution.py:94
  39.7 0.7 slice.58
  40.4 2.1 %collective-permute-start = (bf16[15,128]{1,0:T(8,128)(2,1)S(1)}, bf16[15,128]{1,0:T(8,128)(2,1)S(1)}, u32[]{:S(2)}, u32[]{:S(2)}) collective-permute-start(bf16[15,128]{1,0:T(8,128)(2,1)S(1)} %slice.58), channel_id=1, source_target_pairs={{0,16},{16,32},{32,48},{48,64},{64,80},{80,96},{96,112},{112,128},... | collective-permute-start | bytes 11528 | tf_op jit(solution)/shard_map/ppermute | solution.py:17
  42.7 47.3 %all-gather.5.cloned.1.call-done = bf16[1,512,4096]{2,1,0:T(8,128)(2,1)} async-done(((bf16[1,512,256]{2,1,0:T(8,128)(2,1)}), bf16[1,512,4096]{2,1,0:T(8,128)(2,1)}) %all-gather.5.cloned.1.call-update) | async-done | bytes 4194320 | tf_op jit(solution)/shard_map/all_gather | solution.py:95
  90.0 3.2 %fusion.1 = f32[512]{0:T(512)S(1)} fusion(bf16[1,512,4096]{2,1,0:T(8,128)(2,1)} %all-gather.5.cloned.1.call-done), kind=kLoop, calls=%fused_computation.6 | loop fusion | flops 6290944 | bytes 4196352 | tf_op jit(solution)/shard_map/reduce_sum | solution.py:99
  93.3 0.2 copy-done.1
  93.4 1.3 fusion.8
  94.7 1.3 fusion.17
  96.1 1.5 broadcast_in_dim.167
  97.6 3.9 %all-to-all-start.1 = ((bf16[16,1,512,128]{2,3,1,0:T(8,128)(2,1)}), bf16[16,1,512,128]{2,3,1,0:T(8,128)(2,1)S(1)}, u32[]{:S(2)}, u32[]{:S(2)}) async-start(bf16[16,1,512,128]{2,3,1,0:T(8,128)(2,1)} %broadcast_in_dim.167), calls=%async_computation.1 | async-start | bytes 4194304 | tf_op jit(solution)/shard_map/all_to_all | solution.py:28
  101.7 1.2 fusion.40
  103.0 53.5 %all-to-all-done.1 = bf16[16,1,512,128]{2,3,1,0:T(8,128)(2,1)S(1)} async-done(((bf16[16,1,512,128]{2,3,1,0:T(8,128)(2,1)}), bf16[16,1,512,128]{2,3,1,0:T(8,128)(2,1)S(1)}, u32[]{:S(2)}, u32[]{:S(2)}) %all-to-all-start.1) | async-done | bytes 2097184 | tf_op jit(solution)/shard_map/all_to_all | solution.py:28
  156.4 0.8 fusion.7
  157.2 0.4 copy.40
  157.6 0.5 broadcast.1945
  158.1 2.3 %reduce.3 = bf16[512,256]{1,0:T(8,128)(2,1)S(1)} reduce(bf16[512,1,256]{2,1,0:T(2,128)(2,1)S(1)} %bitcast.65, bf16[]{:T(256)} %broadcast.1945), dimensions={1}, to_apply=%bitcast.60.reduce_sub_computation | reduce | bytes 524290
  160.4 0.8 reshape.278
  161.2 9.5 %all-to-all-start.2 = ((bf16[32,2,2048]{2,1,0:T(2,128)(2,1)}), bf16[32,2,2048]{2,1,0:T(2,128)(2,1)S(1)}, u32[]{:S(2)}, u32[]{:S(2)}) async-start(bf16[32,2,2048]{2,1,0:T(2,128)(2,1)} %reshape.278), calls=%async_computation.2 | async-start | bytes 524288 | tf_op jit(solution)/shard_map/all_to_all | solution.py:108
  170.9 3.3 %convolution_convert_fusion.1 = bf16[512,256]{1,0:T(8,128)(2,1)} fusion(bf16[512,2048]{1,0:T(8,128)(2,1)} %all-gather.3.cloned.1.call-done, bf16[2048,256]{1,0:T(8,128)(2,1)} %param.10), kind=kOutput, calls=%fused_computation.11 | convolution fusion | flops 537001984 | bytes 3407872 | tf_op jit(solution)/shard_map/dot_general | solution.py:78
  174.2 7.0 %all-to-all-done.2 = bf16[32,2,2048]{2,1,0:T(2,128)(2,1)S(1)} async-done(((bf16[32,2,2048]{2,1,0:T(2,128)(2,1)}), bf16[32,2,2048]{2,1,0:T(2,128)(2,1)S(1)}, u32[]{:S(2)}, u32[]{:S(2)}) %all-to-all-start.2) | async-done | bytes 262176 | tf_op jit(solution)/shard_map/all_to_all | solution.py:108
  181.1 0.3 reshape.279
  181.5 1.2 gather_fusion.1
  182.7 1.0 multiply_reduce_fusion
  (49 shorter events, 1.4 us)
Async XLA Ops:
  7.2 149.3 %copy-start = (bf16[1,2048,256]{2,1,0:T(8,128)(2,1)S(1)}, bf16[1,2048,256]{2,1,0:T(8,128)(2,1)}, u32[]{:S(2)}) copy-start(bf16[1,2048,256]{2,1,0:T(8,128)(2,1)} %param.17) | copy-start | bytes 3145732
  7.2 86.1 %copy-start.6 = (f32[4096]{0:T(1024)S(1)}, f32[4096]{0:T(1024)}, u32[]{:S(2)}) copy-start(f32[4096]{0:T(1024)} %param.14) | copy-start | bytes 49156
  7.2 86.1 %copy-start.4 = (bf16[1,4096,128]{2,1,0:T(8,128)(2,1)S(1)}, bf16[1,4096,128]{2,1,0:T(8,128)(2,1)}, u32[]{:S(2)}) copy-start(bf16[1,4096,128]{2,1,0:T(8,128)(2,1)} %param.15) | copy-start | bytes 3145732
  7.2 82.8 %all-gather.5.cloned.1.call-start = ((), (), s32[]{:S(2)}) async-start(), calls=%async_computation.4 | async-start | bytes 4456448 | tf_op jit(solution)/shard_map/all_gather | solution.py:95
  40.4 61.3 %collective-permute-start = (bf16[15,128]{1,0:T(8,128)(2,1)S(1)}, bf16[15,128]{1,0:T(8,128)(2,1)S(1)}, u32[]{:S(2)}, u32[]{:S(2)}) collective-permute-start(bf16[15,128]{1,0:T(8,128)(2,1)S(1)} %slice.58), channel_id=1, source_target_pairs={{0,16},{16,32},{32,48},{48,64},{64,80},{80,96},{96,112},{112,128},... | collective-permute-start | bytes 11528 | tf_op jit(solution)/shard_map/ppermute | solution.py:17
  90.0 3.4 %copy-start.1 = (bf16[1,512,4096]{2,1,0:T(8,128)(2,1)S(1)}, bf16[1,512,4096]{2,1,0:T(8,128)(2,1)}, u32[]{:S(2)}) copy-start(bf16[1,512,4096]{2,1,0:T(8,128)(2,1)} %all-gather.5.cloned.1.call-done) | copy-start | bytes 12582916
  93.2 1.5 copy-start.5
  96.0 5.7 %copy-start.2 = (bf16[512,128]{1,0:T(8,128)(2,1)S(1)}, bf16[512,128]{1,0:T(8,128)(2,1)}, u32[]{:S(2)}) copy-start(bf16[512,128]{1,0:T(8,128)(2,1)} %param.9) | copy-start | bytes 393220
  97.6 5.3 %copy-start.3 = (f32[128,2]{0,1:T(2,128)S(1)}, f32[128,2]{0,1:T(2,128)}, u32[]{:S(2)}) copy-start(f32[128,2]{0,1:T(2,128)} %param.13) | copy-start | bytes 3076
  97.6 58.8 %all-to-all-start.1 = ((bf16[16,1,512,128]{2,3,1,0:T(8,128)(2,1)}), bf16[16,1,512,128]{2,3,1,0:T(8,128)(2,1)S(1)}, u32[]{:S(2)}, u32[]{:S(2)}) async-start(bf16[16,1,512,128]{2,3,1,0:T(8,128)(2,1)} %broadcast_in_dim.167), calls=%async_computation.1 | async-start | bytes 4194304 | tf_op jit(solution)/shard_map/all_to_all | solution.py:28
  101.5 69.4 %all-gather.3.cloned.1.call-start = ((), (), s32[]{:S(2)}) async-start(), calls=%async_computation.3 | async-start | bytes 2228224 | tf_op jit(solution)/shard_map/all_gather | solution.py:79
  161.2 19.9 %all-to-all-start.2 = ((bf16[32,2,2048]{2,1,0:T(2,128)(2,1)}), bf16[32,2,2048]{2,1,0:T(2,128)(2,1)S(1)}, u32[]{:S(2)}, u32[]{:S(2)}) async-start(bf16[32,2,2048]{2,1,0:T(2,128)(2,1)} %reshape.278), calls=%async_computation.2 | async-start | bytes 524288 | tf_op jit(solution)/shard_map/all_to_all | solution.py:108
Sparse Core Ops, SparseCore 0:
  39.8 50.1 all-gather.4
  105.0 63.7 all-gather.2
where the time goes:
time: 192 us; the launch traced here: 191 us
  waiting for transfers between devices  108 us (56%)
  blocking collectives  24.9 us (13%)
  starting transfers between devices  15.6 us (8%)
  between operations  14.3 us (7%)
  local copies, waits for them, and re-layouts  11.8 us (6%)
  other arithmetic  9.6 us (5%)
  matrix products  6.55 us (3%)
    all_to_all x1, waiting for transfers between devices, copy_for_each(): lax.all_to_all(jnp.broadcast_to(value[None], (size, *value.shape)), axis,...  53.5 us
    all_gather x1, waiting for transfers between devices, shards(): portion = lax.all_gather(arrived, 'tp', axis=2, tiled=True)  47.3 us
    all_to_all x1, blocking collectives, shards(): lax.all_to_all(outgoing, 'ep', split_axis=0, concat_axis=1, tiled=True)  24.9 us
    all_to_all x1, starting transfers between devices, shards(): lax.all_to_all(produced, 'ep', split_axis=1, concat_axis=0, tiled=True)  9.53 us
    all_to_all x1, waiting for transfers between devices, shards(): lax.all_to_all(produced, 'ep', split_axis=1, concat_axis=0, tiled=True)  6.97 us
    all_to_all x1, starting transfers between devices, copy_for_each(): lax.all_to_all(jnp.broadcast_to(value[None], (size, *value.shape)), axis,...  3.91 us
  transfers between devices with their start and end apart: 5, of which 3 were waited for; matrix products, arithmetic and copies ran while one was open for 9% of the time, Pallas kernels for 0%

commit v1 on v0

v1 whole, which is shorter than its diff:
```python
import functools

import jax
import jax.numpy as jnp
from jax import lax
from jax.experimental import pallas as pl
from jax.experimental.pallas import tpu as pltpu
from jax.sharding import PartitionSpec as P

MESH = pl.DeviceIdType.MESH
TOP = 2
REACH = 16
EPS = 1e-06
CHUNKS = 2
MIX_PIECES = 4


class Stream:
    def __init__(self, buf, pieces, groups, send, recv, mate_send, mate_recv):
        self.buf = buf
        self.pieces = pieces
        self.groups = groups
        self.per_group = pieces // groups
        self.rows = buf.shape[2] // pieces
        self.send, self.recv, self.mate_send, self.mate_recv = send, recv, mate_send, mate_recv


def kernel(
    ep_size,
    tp_size,
    group_size,
    order,
    mix_in,
    x_in,
    index_in,
    share_in,
    gain_in,
    mix_w,
    gate_w,
    up_w,
    down_w,
    mixed_out,
    rows_out,
    mw,
    wgu,
    wd,
    ext,
    halo,
    pg,
    tg,
    hg,
    outgoing,
    produced,
    returned,
    acc_m,
    acc_t,
    acc_d,
    squares,
    columns,
    w_sem,
    halo_sem,
    disp_send,
    disp_recv,
    ret_send,
    ret_recv,
    m_send,
    m_recv,
    m_mate_send,
    m_mate_recv,
    t_send,
    t_recv,
    t_mate_send,
    t_mate_recv,
    h_send,
    h_recv,
    h_mate_send,
    h_mate_recv,
):
    ep = lax.axis_index("ep")
    tp = lax.axis_index("tp")
    ny = tp_size // 2
    half = ny // 2
    core = lax.rem(tp, 2)
    y = tp // 2
    up = lax.rem(tp + 2, tp_size)
    down = lax.rem(tp + tp_size - 2, tp_size)
    mate = tp + 1 - 2 * core
    tokens, feats = x_in.shape
    length, chans = mix_in.shape
    slots = outgoing.shape[0]
    cap = slots // ep_size
    hid = hg.shape[3]
    chunk_rows = slots // CHUNKS
    in_chunk = ep_size // CHUNKS

    mix = Stream(pg, MIX_PIECES, 1, m_send, m_recv, m_mate_send, m_mate_recv)
    tok = Stream(tg, 2 * CHUNKS, CHUNKS, t_send, t_recv, t_mate_send, t_mate_recv)
    hdn = Stream(hg, 2 * CHUNKS, CHUNKS, h_send, h_recv, h_mate_send, h_mate_recv)

    def place(source):
        return lax.rem(source, CHUNKS) * in_chunk + source // CHUNKS

    def block(i):
        return pl.ds(pl.multiple_of(i * cap, cap), cap)

    w_copies = [
        pltpu.make_async_copy(mix_w, mw, w_sem.at[0]),
        pltpu.make_async_copy(gate_w, wgu.at[:, pl.ds(0, hid)], w_sem.at[1]),
        pltpu.make_async_copy(up_w, wgu.at[:, pl.ds(hid, hid)], w_sem.at[2]),
        pltpu.make_async_copy(down_w, wd, w_sem.at[3]),
    ]
    for copy in w_copies:
        copy.start()

    barrier = pltpu.get_barrier_semaphore()
    for other in (up, down, mate):
        pl.semaphore_signal(barrier, inc=1, device_id=(ep, other), device_id_type=MESH)

    def greet(i, carry):
        pl.semaphore_signal(
            barrier, inc=1, device_id=(lax.rem(ep + i, ep_size), tp), device_id_type=MESH
        )
        return carry

    lax.fori_loop(1, ep_size, greet, 0)

    expert_rows = lax.broadcasted_iota(jnp.int32, (ep_size, tokens), 0)
    named = [index_in[k : k + 1, :] for k in range(TOP)]
    hits = [(expert_rows == named[k]).astype(jnp.float32) for k in range(TOP)]
    before = (
        lax.broadcasted_iota(jnp.int32, (tokens, tokens), 0)
        < lax.broadcasted_iota(jnp.int32, (tokens, tokens), 1)
    ).astype(jnp.bfloat16)
    earlier = jnp.dot(
        (hits[0] + hits[1]).astype(jnp.bfloat16), before, preferred_element_type=jnp.float32
    )
    ranks = [
        jnp.sum(earlier * hits[0], axis=0, keepdims=True),
        jnp.sum((earlier + hits[0]) * hits[1], axis=0, keepdims=True),
    ]
    targets = [named[k] * cap + ranks[k].astype(jnp.int32) for k in range(TOP)]
    slot_rows = lax.broadcasted_iota(jnp.int32, (slots, tokens), 0)
    picks = jnp.logical_or(slot_rows == targets[0], slot_rows == targets[1])
    outgoing[...] = jnp.dot(
        picks.astype(jnp.bfloat16), x_in[...], preferred_element_type=jnp.float32
    ).astype(jnp.bfloat16)
    total_share = share_in[0:1, :] + share_in[1:2, :]
    row_id = lax.broadcasted_iota(jnp.int32, (tokens, tokens), 0)
    packed = jnp.zeros((tokens, tokens), jnp.float32)
    packed = jnp.where(row_id == 0, targets[0].astype(jnp.float32), packed)
    packed = jnp.where(row_id == 1, targets[1].astype(jnp.float32), packed)
    packed = jnp.where(row_id == 2, share_in[0:1, :] / total_share, packed)
    packed = jnp.where(row_id == 3, share_in[1:2, :] / total_share, packed)
    columns[...] = packed.T

    ext[pl.ds(REACH, length), :] = mix_in[...].astype(jnp.float32)
    group = (tp * chans) // group_size
    window = jnp.where(group == 0, 2, jnp.where(group == 1, 4, jnp.where(group == 2, 8, 16)))

    def window_sum(first, count):
        running = ext[pl.ds(REACH + first, count), :]
        for lag in range(1, REACH):
            running = running + jnp.where(
                lag < window, ext[pl.ds(REACH + first - lag, count), :], 0.0
            )
        return running

    inverse_window = jnp.where(
        group == 0, 0.5, jnp.where(group == 1, 0.25, jnp.where(group == 2, 0.125, 0.0625))
    )
    step = min(64, length // MIX_PIECES)
    for first in range(0, length, step):
        skip = REACH if first == 0 else 0
        at, count = first + skip, step - skip
        if count:
            pg[y, core, pl.ds(at, count), :] = (
                window_sum(at, count) * inverse_window - ext[pl.ds(REACH + at, count), :]
            ).astype(jnp.bfloat16)

    pl.semaphore_wait(barrier, ep_size - 1 + 3)

    halo_copy = pltpu.make_async_remote_copy(
        src_ref=mix_in.at[pl.ds(length - REACH, REACH), :],
        dst_ref=halo,
        send_sem=halo_sem.at[0],
        recv_sem=halo_sem.at[1],
        device_id=(lax.rem(ep + 1, ep_size), tp),
        device_id_type=MESH,
    )
    halo_copy.start()

    def dispatch(i, carry):
        other = lax.rem(ep + i, ep_size)
        pltpu.make_async_remote_copy(
            src_ref=outgoing.at[block(other), :],
            dst_ref=tg.at[y, core, block(place(ep)), :],
            send_sem=disp_send,
            recv_sem=disp_recv.at[lax.rem(ep, CHUNKS)],
            device_id=(other, tp),
            device_id_type=MESH,
        ).start()
        return carry

    def limit(piece, way):
        return half if (piece % 2 == 0) == (way == 0) else half - 1

    def part(stream, origin, piece):
        return stream.buf.at[origin, core, pl.ds(piece * stream.rows, stream.rows), :]

    def ring_send(stream, piece, way, origin, hop):
        ref = part(stream, origin, piece)
        pltpu.make_async_remote_copy(
            src_ref=ref,
            dst_ref=ref,
            send_sem=stream.send.at[piece],
            recv_sem=stream.recv.at[piece, way, hop],
            device_id=(ep, up if way == 0 else down),
            device_id_type=MESH,
        ).start()

    def mate_copy(stream, piece, origin, hop):
        ref = part(stream, origin, piece)
        pltpu.make_async_remote_copy(
            src_ref=ref,
            dst_ref=ref,
            send_sem=stream.mate_send.at[piece],
            recv_sem=stream.mate_recv.at[piece // stream.per_group, hop],
            device_id=(ep, mate),
            device_id_type=MESH,
        ).start()

    def origin_of(way, hop):
        return lax.rem(y + ny - hop, ny) if way == 0 else lax.rem(y + hop, ny)

    def move(stream, piece, hop):
        if hop == 0:
            for way in range(2):
                if limit(piece, way) > 0:
                    ring_send(stream, piece, way, y, 0)
            mate_copy(stream, piece, y, 0)
            return
        for way in range(2):
            if hop > limit(piece, way):
                continue
            origin = origin_of(way, hop)
            ref = part(stream, origin, piece)
            pltpu.make_async_copy(ref, ref, stream.recv.at[piece, way, hop - 1]).wait()
            if hop < limit(piece, way):
                ring_send(stream, piece, way, origin, hop)
            mate_copy(stream, piece, origin, hop)

    def mate_wait(stream, group_no, hop):
        rows = stream.rows * stream.per_group
        if 0 < hop < half:
            ref = stream.buf.at[pl.ds(0, 2), 0, pl.ds(0, rows), :]
        else:
            ref = stream.buf.at[0, 0, pl.ds(0, rows), :]
        pltpu.make_async_copy(ref, ref, stream.mate_recv.at[group_no, hop]).wait()

    def for_origins(hop, item):
        if hop == 0:
            item(y)
        elif hop == half:
            item(origin_of(0, hop))
        else:

            def both(way, carry):
                item(lax.rem(y + ny + (2 * way - 1) * hop, ny))
                return carry

            lax.fori_loop(0, 2, both, 0)

    def mix_item(first):
        def item(origin):
            a = jnp.concatenate([pg[origin, 0], pg[origin, 1]], axis=1)
            rows = pl.ds(pl.multiple_of(origin * 2 * chans, 2 * chans), 2 * chans)
            got = jnp.dot(a, mw[rows, :], preferred_element_type=jnp.float32)
            acc_m[...] = got if first else acc_m[...] + got

        return item

    def token_item(ch, first):
        at = pl.ds(ch * chunk_rows, chunk_rows)

        def item(origin):
            scaled, sums = [], 0.0
            for j in range(2):
                x = tg[origin, j, at, :].astype(jnp.float32)
                lanes = pl.ds(pl.multiple_of((origin * 2 + j) * feats, feats), feats)
                scaled.append((x * gain_in[:, lanes]).astype(jnp.bfloat16))
                sq = x * x
                for q in range(0, feats, 128):
                    sums = sums + sq[:, q : q + 128]
            rows = pl.ds(pl.multiple_of(origin * 2 * feats, 2 * feats), 2 * feats)
            got = jnp.dot(
                jnp.concatenate(scaled, axis=1), wgu[rows, :], preferred_element_type=jnp.float32
            )
            if first:
                acc_t[at, :] = got
                squares[at, :] = sums
            else:
                acc_t[at, :] = acc_t[at, :] + got
                squares[at, :] = squares[at, :] + sums

        return item

    def down_item(ch, first):
        at = pl.ds(ch * chunk_rows, chunk_rows)

        def item(origin):
            a = jnp.concatenate([hg[origin, 0, at, :], hg[origin, 1, at, :]], axis=1)
            rows = pl.ds(pl.multiple_of(origin * 2 * hid, 2 * hid), 2 * hid)
            got = jnp.dot(a, wd[rows, :], preferred_element_type=jnp.float32)
            acc_d[at, :] = got if first else acc_d[at, :] + got

        return item

    def activate(ch):
        at = pl.ds(ch * chunk_rows, chunk_rows)
        total = jnp.sum(squares[at, :], axis=1, keepdims=True)
        inverse = lax.rsqrt(total / (feats * tp_size) + EPS)
        gate = acc_t[at, pl.ds(0, hid)] * inverse
        upper = acc_t[at, pl.ds(hid, hid)] * inverse
        hg[y, core, at, :] = (gate / (1.0 + jnp.exp(-gate)) * upper).astype(jnp.bfloat16)

    def dispatched(ch):
        mine = lax.rem(ep, CHUNKS) == ch
        base = ch * chunk_rows

        @pl.when(mine)
        def _():
            if in_chunk > 1:
                ref = tg.at[0, 0, pl.ds(base, chunk_rows - cap), :]
                pltpu.make_async_copy(ref, ref, disp_recv.at[ch]).wait()
            tg[y, core, block(place(ep)), :] = outgoing[block(ep), :]

        @pl.when(jnp.logical_not(mine))
        def _():
            ref = tg.at[0, 0, pl.ds(base, chunk_rows), :]
            pltpu.make_async_copy(ref, ref, disp_recv.at[ch]).wait()

    def give_back(ch):
        at = pl.ds(ch * chunk_rows, chunk_rows)
        produced[at, :] = acc_d[at, :].astype(jnp.bfloat16)

        def one(i, carry):
            other = lax.rem(ep + i, ep_size)

            @pl.when(lax.rem(other, CHUNKS) == ch)
            def _():
                pltpu.make_async_remote_copy(
                    src_ref=produced.at[block(place(other)), :],
                    dst_ref=returned.at[block(ep), :],
                    send_sem=ret_send,
                    recv_sem=ret_recv,
                    device_id=(other, tp),
                    device_id_type=MESH,
                ).start()

            return carry

        lax.fori_loop(1, ep_size, one, 0)

        @pl.when(lax.rem(ep, CHUNKS) == ch)
        def _():
            returned[block(ep), :] = produced[block(place(ep)), :]

    def first_rows():
        halo_copy.wait_recv()
        ext[pl.ds(0, REACH), :] = jnp.where(ep == 0, 0.0, halo[...].astype(jnp.float32))
        position = ep * length + lax.broadcasted_iota(jnp.int32, (REACH, chans), 0)
        counts = jnp.minimum(position + 1, window).astype(jnp.float32)
        pg[y, core, pl.ds(0, REACH), :] = (
            window_sum(0, REACH) / counts - ext[pl.ds(REACH, REACH), :]
        ).astype(jnp.bfloat16)

    streams = {"m": mix, "t": tok, "h": hdn}
    for entry in order:
        kind = entry[0]
        if kind in streams:
            move(streams[kind], entry[1], entry[2])
        elif kind == "disp":
            lax.fori_loop(1, ep_size, dispatch, 0)
        elif kind == "first":
            first_rows()
        elif kind == "got":
            dispatched(entry[1])
        elif kind == "w":
            w_copies[entry[1]].wait()
        elif kind == "mc":
            mate_wait(mix, 0, entry[1])
            for_origins(entry[1], mix_item(entry[1] == 0))
        elif kind == "mo":
            mixed_out[...] = acc_m[...].astype(jnp.bfloat16)
        elif kind == "tc":
            mate_wait(tok, entry[1], entry[2])
            for_origins(entry[2], token_item(entry[1], entry[2] == 0))
        elif kind == "act":
            activate(entry[1])
        elif kind == "dc":
            mate_wait(hdn, entry[1], entry[2])
            for_origins(entry[2], down_item(entry[1], entry[2] == 0))
        elif kind == "ret":
            give_back(entry[1])

    halo_copy.wait_send()
    others = pl.ds(0, slots - cap)
    pltpu.make_async_copy(outgoing.at[others, :], outgoing.at[others, :], disp_send).wait()
    pltpu.make_async_copy(produced.at[others, :], produced.at[others, :], ret_send).wait()
    for stream in streams.values():
        for piece in range(stream.pieces):
            ref = stream.buf.at[pl.ds(0, ny - 1), 0, pl.ds(0, stream.rows), :]
            pltpu.make_async_copy(ref, ref, stream.send.at[piece]).wait()
            ref = stream.buf.at[pl.ds(0, ny), 0, pl.ds(0, stream.rows), :]
            pltpu.make_async_copy(ref, ref, stream.mate_send.at[piece]).wait()

    slot_lanes = lax.broadcasted_iota(jnp.int32, (tokens, slots), 1)
    takes = [
        (columns[:, k : k + 1].astype(jnp.int32) == slot_lanes).astype(jnp.bfloat16)
        for k in range(TOP)
    ]
    pltpu.make_async_copy(returned.at[others, :], returned.at[others, :], ret_recv).wait()
    rows = 0.0
    for k in range(TOP):
        picked = jnp.dot(takes[k], returned[...], preferred_element_type=jnp.float32)
        rows = rows + picked * columns[:, TOP + k : TOP + k + 1]
    rows_out[...] = rows.astype(jnp.bfloat16)


def full_order(half):
    m = [1, 2, 3, 0]
    order = [("m", 1, 0), ("m", 2, 0), ("m", 3, 0), ("disp",), ("first",), ("m", 0, 0)]
    for hop in (1, 2):
        order += [("m", p, hop) for p in m if hop <= half]
    order += [("got", 0), ("t", 0, 0), ("t", 1, 0)]
    for hop in range(3, half + 1):
        order += [("m", p, hop) for p in m]
    order += [("w", 0), ("mc", 0)]
    order += [("got", 1)]

    def t(ch, hop):
        return [("t", 2 * ch, hop), ("t", 2 * ch + 1, hop)]

    def h(ch, hop):
        return [("h", 2 * ch, hop), ("h", 2 * ch + 1, hop)]

    late = [("mc", hop) for hop in range(1, half + 1)] + [("mo",)]
    order += [("w", 1), ("w", 2)]
    if half == 4:
        order += t(0, 1) + [("t", 2, 0), late[0], ("tc", 0, 0)]
        order += t(0, 2) + [("t", 3, 0), late[1], ("tc", 0, 1)]
        order += t(0, 3) + [("t", 2, 1), late[2], ("tc", 0, 2)]
        order += t(0, 4) + [("t", 3, 1), ("tc", 0, 3), ("t", 2, 2), ("tc", 0, 4), ("act", 0)]
        order += [("h", 0, 0), ("h", 1, 0), ("t", 3, 2), ("tc", 1, 0), ("h", 0, 1), ("t", 2, 3)]
        order += [("h", 1, 1), ("t", 3, 3), late[3], late[4], ("tc", 1, 1), ("w", 3), ("dc", 0, 0)]
        order += h(0, 2) + [("tc", 1, 2), ("dc", 0, 1)] + t(1, 4)
        order += [("tc", 1, 3)] + h(0, 3) + [("tc", 1, 4), ("act", 1)]
        order += h(1, 0) + [("dc", 0, 2)] + h(0, 4) + h(1, 1)
        order += [("dc", 0, 3), ("dc", 0, 4), ("ret", 0)]
        order += h(1, 2) + [("dc", 1, 0)] + h(1, 3) + [("dc", 1, 1)] + h(1, 4)
        order += [("dc", 1, 2), ("dc", 1, 3), ("dc", 1, 4), ("ret", 1)]
    else:
        order += t(1, 0)
        for ch in range(CHUNKS):
            for hop in range(1, half + 1):
                order += t(ch, hop)
            order += [("tc", ch, hop) for hop in range(half + 1)] + [("act", ch)]
        order += late + [("w", 3)]
        for ch in range(CHUNKS):
            order += h(ch, 0)
        for ch in range(CHUNKS):
            for hop in range(1, half + 1):
                order += h(ch, hop)
            order += [("dc", ch, hop) for hop in range(half + 1)] + [("ret", ch)]
    return order


def solution(mesh):
    ep_size, tp_size = mesh.shape["ep"], mesh.shape["tp"]
    ny = tp_size // 2
    half = ny // 2

    def shards(mix_input, mix_weight, expert_input, expert_index, route_share, norm_gain, gate_weight, up_weight, down_weight):
        length, chans = mix_input.shape
        tokens, feats = expert_input.shape
        slots = 2 * tokens * TOP
        width = mix_weight.shape[1]
        hid = gate_weight.shape[2]
        vmem, dma = pltpu.VMEM, pltpu.SemaphoreType.DMA
        bf16, f32 = jnp.bfloat16, jnp.float32

        def stream_sems(pieces, groups):
            return [dma((pieces,)), dma((pieces, 2, half)), dma((pieces,)), dma((groups, half + 1))]

        here = pl.BlockSpec(memory_space=pltpu.VMEM)
        there = pl.BlockSpec(memory_space=pl.ANY)
        flops = 2 * (length * chans * tp_size * width + slots * (feats * tp_size * 2 * hid + hid * tp_size * width))
        call = pl.pallas_call(
            functools.partial(
                kernel, ep_size, tp_size, chans * tp_size // 4, full_order(half)
            ),
            name="mixer_and_experts",
            out_shape=(
                jax.ShapeDtypeStruct((length, width), bf16),
                jax.ShapeDtypeStruct((tokens, width), bf16),
            ),
            in_specs=[here] * 5 + [there] * 4,
            out_specs=(here, here),
            scratch_shapes=[
                vmem(mix_weight.shape, bf16),
                vmem((feats * tp_size, 2 * hid), bf16),
                vmem(down_weight.shape[1:], bf16),
                vmem((length + REACH, chans), f32),
                vmem((REACH, chans), bf16),
                vmem((ny, 2, length, chans), bf16),
                vmem((ny, 2, slots, feats), bf16),
                vmem((ny, 2, slots, hid), bf16),
                vmem((slots, feats), bf16),
                vmem((slots, width), bf16),
                vmem((slots, width), bf16),
                vmem((length, width), f32),
                vmem((slots, 2 * hid), f32),
                vmem((slots, width), f32),
                vmem((slots, 128), f32),
                vmem((tokens, tokens), f32),
                dma((4,)),
                dma((2,)),
                dma,
                dma((CHUNKS,)),
                dma,
                dma,
            ]
            + stream_sems(MIX_PIECES, 1)
            + stream_sems(2 * CHUNKS, CHUNKS)
            + stream_sems(2 * CHUNKS, CHUNKS),
            compiler_params=pltpu.CompilerParams(
                collective_id=0, has_side_effects=True, vmem_limit_bytes=60 * 1024 * 1024
            ),
            cost_estimate=pl.CostEstimate(flops=flops, bytes_accessed=8 * 1024 * 1024, transcendentals=0),
        )
        return call(
            mix_input,
            expert_input,
            expert_index.T,
            route_share.T,
            norm_gain.reshape(1, -1),
            mix_weight,
            gate_weight[0],
            up_weight[0],
            down_weight[0],
        )

    placed = (
        P("ep", "tp"),
        P(None, "tp"),
        P("ep", "tp"),
        P("ep", None),
        P("ep", None),
        P(),
        P("ep", None, "tp"),
        P("ep", None, "tp"),
        P("ep", None, "tp"),
    )
    return jax.shard_map(
        shards,
        mesh=mesh,
        in_specs=placed,
        out_specs=(P("ep", "tp"), P("ep", "tp")),
        check_vma=False,
    )
```

time: 192 us -> 89 us (0.46)
  the two profiles are of different devices: /device:TPU:1 before, /device:TPU:14 now
where the time goes in v1:
time: 89 us; the launch traced here: 88.9 us
  Pallas kernels  85.9 us (97%)
  local copies, waits for them, and re-layouts  2.33 us (3%)
    pallas_call x1, Pallas kernels, shards(): call(mix_input, expert_input, expert_index.T, route_share.T, norm_gain.re...  85.9 us
    unnamed x4, local copies, waits for them, and re-layouts  2.33 us

profile of v1, /device:TPU:14, one launch (start us, length us, event | category | flops | bytes accessed | tf_op | source)
XLA Modules:
  0.0 88.9 jit_solution(13922189899592881693)
XLA Ops:
  0.6 85.9 %mixer_and_experts.1 = (bf16[512,256]{1,0:T(8,128)(2,1)}, bf16[128,256]{1,0:T(8,128)(2,1)}) custom-call(bf16[512,128]{1,0:T(8,128)(2,1)} %mix_in.1, bf16[128,256]{1,0:T(8,128)(2,1)} %x_in.1, s32[2,128]{1,0:T(2,128)} %bitcast.10, f32[2,128]{1,0:T(2,128)} %bitcast.11, f32[1,4096]{1,0:T(1,128)} %bitcast.9, bf16[2048,256]{1,0:T(8,128)(2,1)} %mix_w.1, ...), custom_call_target="tpu_custom_call" | custom-call | flops 2147483648 | bytes 8388608 | tf_op jit(solution)/shard_map/mixer_and_experts/pallas_call | solution.py:541
  86.5 0.0 copy-start
  86.6 1.7 %copy.13 = bf16[512,256]{1,0:T(8,128)(2,1)} copy(bf16[512,256]{1,0:T(8,128)(2,1)} %get-tuple-element.4) | data formatting | bytes 524288
  88.3 0.0 copy-done
  88.3 0.6 copy.14
Async XLA Ops:
  86.5 1.7 %copy-start = (bf16[128,256]{1,0:T(8,128)(2,1)S(1)}, bf16[128,256]{1,0:T(8,128)(2,1)}, u32[]{:S(2)}) copy-start(bf16[128,256]{1,0:T(8,128)(2,1)} %get-tuple-element.5) | copy-start | bytes 196612

commit v2 on v1

--- a/solution.py
+++ b/solution.py
@@ -11,36 +11,46 @@
 TOP = 2
 REACH = 16
 EPS = 1e-06
-CHUNKS = 2
-MIX_PIECES = 4
+MIX_GROUPS = 2
 
 
 class Stream:
-    def __init__(self, buf, pieces, groups, send, recv, mate_send, mate_recv):
+    def __init__(self, buf, group_rows, sems):
         self.buf = buf
-        self.pieces = pieces
-        self.groups = groups
-        self.per_group = pieces // groups
-        self.rows = buf.shape[2] // pieces
-        self.send, self.recv, self.mate_send, self.mate_recv = send, recv, mate_send, mate_recv
+        self.group_rows = group_rows
+        self.group_first = [sum(group_rows[:g]) for g in range(len(group_rows))]
+        self.send, self.recv, self.mate_send, self.mate_recv = sems
+
+    def group(self, g):
+        return pl.ds(self.group_first[g], self.group_rows[g])
+
+    def rows(self, piece):
+        size = self.group_rows[piece // 2] // 2
+        return self.group_first[piece // 2] + (piece % 2) * size, size
 
 
 def kernel(
     ep_size,
     tp_size,
     group_size,
+    sources,
     order,
-    mix_in,
-    x_in,
-    index_in,
-    share_in,
-    gain_in,
+    mix_hbm,
+    x_hbm,
+    index_hbm,
+    share_hbm,
+    gain_hbm,
     mix_w,
     gate_w,
     up_w,
     down_w,
     mixed_out,
     rows_out,
+    mix_in,
+    x_in,
+    index_in,
+    share_in,
+    gain_in,
     mw,
     wgu,
     wd,
@@ -57,6 +67,7 @@
     acc_d,
     squares,
     columns,
+    in_sem,
     w_sem,
     halo_sem,
     disp_send,
@@ -90,19 +101,30 @@
     slots = outgoing.shape[0]
     cap = slots // ep_size
     hid = hg.shape[3]
-    chunk_rows = slots // CHUNKS
-    in_chunk = ep_size // CHUNKS
-
-    mix = Stream(pg, MIX_PIECES, 1, m_send, m_recv, m_mate_send, m_mate_recv)
-    tok = Stream(tg, 2 * CHUNKS, CHUNKS, t_send, t_recv, t_mate_send, t_mate_recv)
-    hdn = Stream(hg, 2 * CHUNKS, CHUNKS, h_send, h_recv, h_mate_send, h_mate_recv)
-
-    def place(source):
-        return lax.rem(source, CHUNKS) * in_chunk + source // CHUNKS
+    chunks = [n * cap for n in sources]
+    bounds = [sum(sources[:ch]) for ch in range(len(sources) + 1)]
+
+    mix = Stream(pg, [length // MIX_GROUPS] * MIX_GROUPS, (m_send, m_recv, m_mate_send, m_mate_recv))
+    tok = Stream(tg, chunks, (t_send, t_recv, t_mate_send, t_mate_recv))
+    hdn = Stream(hg, chunks, (h_send, h_recv, h_mate_send, h_mate_recv))
 
     def block(i):
         return pl.ds(pl.multiple_of(i * cap, cap), cap)
 
+    in_copies = [
+        pltpu.make_async_copy(src, dst, in_sem.at[i])
+        for i, (src, dst) in enumerate(
+            (
+                (index_hbm, index_in),
+                (x_hbm, x_in),
+                (share_hbm, share_in),
+                (mix_hbm, mix_in),
+                (gain_hbm, gain_in),
+            )
+        )
+    ]
+    for copy in in_copies:
+        copy.start()
     w_copies = [
         pltpu.make_async_copy(mix_w, mw, w_sem.at[0]),
         pltpu.make_async_copy(gate_w, wgu.at[:, pl.ds(0, hid)], w_sem.at[1]),
@@ -123,6 +145,9 @@
         return carry
 
     lax.fori_loop(1, ep_size, greet, 0)
+
+    for copy in in_copies:
+        copy.wait()
 
     expert_rows = lax.broadcasted_iota(jnp.int32, (ep_size, tokens), 0)
     named = [index_in[k : k + 1, :] for k in range(TOP)]
@@ -168,14 +193,15 @@
     inverse_window = jnp.where(
         group == 0, 0.5, jnp.where(group == 1, 0.25, jnp.where(group == 2, 0.125, 0.0625))
     )
-    step = min(64, length // MIX_PIECES)
-    for first in range(0, length, step):
-        skip = REACH if first == 0 else 0
-        at, count = first + skip, step - skip
-        if count:
-            pg[y, core, pl.ds(at, count), :] = (
-                window_sum(at, count) * inverse_window - ext[pl.ds(REACH + at, count), :]
-            ).astype(jnp.bfloat16)
+    def pool(piece):
+        at, size = mix.rows(piece)
+        for first in range(at, at + size, min(64, size)):
+            skip = REACH if first == 0 else 0
+            begin, count = first + skip, min(64, size) - skip
+            if count:
+                pg[y, core, pl.ds(begin, count), :] = (
+                    window_sum(begin, count) * inverse_window - ext[pl.ds(REACH + begin, count), :]
+                ).astype(jnp.bfloat16)
 
     pl.semaphore_wait(barrier, ep_size - 1 + 3)
 
@@ -189,13 +215,17 @@
     )
     halo_copy.start()
 
+    my_chunk = 0
+    for bound in bounds[1:-1]:
+        my_chunk = my_chunk + jnp.where(ep >= bound, 1, 0)
+
     def dispatch(i, carry):
         other = lax.rem(ep + i, ep_size)
         pltpu.make_async_remote_copy(
             src_ref=outgoing.at[block(other), :],
-            dst_ref=tg.at[y, core, block(place(ep)), :],
+            dst_ref=tg.at[y, core, block(ep), :],
             send_sem=disp_send,
-            recv_sem=disp_recv.at[lax.rem(ep, CHUNKS)],
+            recv_sem=disp_recv.at[my_chunk],
             device_id=(other, tp),
             device_id_type=MESH,
         ).start()
@@ -205,7 +235,7 @@
         return half if (piece % 2 == 0) == (way == 0) else half - 1
 
     def part(stream, origin, piece):
-        return stream.buf.at[origin, core, pl.ds(piece * stream.rows, stream.rows), :]
+        return stream.buf.at[origin, core, pl.ds(*stream.rows(piece)), :]
 
     def ring_send(stream, piece, way, origin, hop):
         ref = part(stream, origin, piece)
@@ -224,7 +254,7 @@
             src_ref=ref,
             dst_ref=ref,
             send_sem=stream.mate_send.at[piece],
-            recv_sem=stream.mate_recv.at[piece // stream.per_group, hop],
+            recv_sem=stream.mate_recv.at[piece // 2, hop],
             device_id=(ep, mate),
             device_id_type=MESH,
         ).start()
@@ -250,7 +280,7 @@
             mate_copy(stream, piece, origin, hop)
 
     def mate_wait(stream, group_no, hop):
-        rows = stream.rows * stream.per_group
+        rows = stream.group_rows[group_no]
         if 0 < hop < half:
             ref = stream.buf.at[pl.ds(0, 2), 0, pl.ds(0, rows), :]
         else:
@@ -270,17 +300,19 @@
 
             lax.fori_loop(0, 2, both, 0)
 
-    def mix_item(first):
+    def mix_item(g, first):
+        at = mix.group(g)
+
         def item(origin):
-            a = jnp.concatenate([pg[origin, 0], pg[origin, 1]], axis=1)
+            a = jnp.concatenate([pg[origin, 0, at, :], pg[origin, 1, at, :]], axis=1)
             rows = pl.ds(pl.multiple_of(origin * 2 * chans, 2 * chans), 2 * chans)
             got = jnp.dot(a, mw[rows, :], preferred_element_type=jnp.float32)
-            acc_m[...] = got if first else acc_m[...] + got
+            acc_m[at, :] = got if first else acc_m[at, :] + got
 
         return item
 
     def token_item(ch, first):
-        at = pl.ds(ch * chunk_rows, chunk_rows)
+        at = tok.group(ch)
 
         def item(origin):
             scaled, sums = [], 0.0
@@ -305,7 +337,7 @@
         return item
 
     def down_item(ch, first):
-        at = pl.ds(ch * chunk_rows, chunk_rows)
+        at = tok.group(ch)
 
         def item(origin):
             a = jnp.concatenate([hg[origin, 0, at, :], hg[origin, 1, at, :]], axis=1)
@@ -316,40 +348,43 @@
         return item
 
     def activate(ch):
-        at = pl.ds(ch * chunk_rows, chunk_rows)
+        at = tok.group(ch)
         total = jnp.sum(squares[at, :], axis=1, keepdims=True)
         inverse = lax.rsqrt(total / (feats * tp_size) + EPS)
         gate = acc_t[at, pl.ds(0, hid)] * inverse
         upper = acc_t[at, pl.ds(hid, hid)] * inverse
         hg[y, core, at, :] = (gate / (1.0 + jnp.exp(-gate)) * upper).astype(jnp.bfloat16)
 
+    def inside(device, ch):
+        return jnp.logical_and(device >= bounds[ch], device < bounds[ch + 1])
+
     def dispatched(ch):
-        mine = lax.rem(ep, CHUNKS) == ch
-        base = ch * chunk_rows
+        base, rows = tok.group_first[ch], chunks[ch]
+        mine = inside(ep, ch)
 
         @pl.when(mine)
         def _():
-            if in_chunk > 1:
-                ref = tg.at[0, 0, pl.ds(base, chunk_rows - cap), :]
+            if rows > cap:
+                ref = tg.at[0, 0, pl.ds(base, rows - cap), :]
                 pltpu.make_async_copy(ref, ref, disp_recv.at[ch]).wait()
-            tg[y, core, block(place(ep)), :] = outgoing[block(ep), :]
+            tg[y, core, block(ep), :] = outgoing[block(ep), :]
 
         @pl.when(jnp.logical_not(mine))
         def _():
-            ref = tg.at[0, 0, pl.ds(base, chunk_rows), :]
+            ref = tg.at[0, 0, pl.ds(base, rows), :]
             pltpu.make_async_copy(ref, ref, disp_recv.at[ch]).wait()
 
     def give_back(ch):
-        at = pl.ds(ch * chunk_rows, chunk_rows)
+        at = tok.group(ch)
         produced[at, :] = acc_d[at, :].astype(jnp.bfloat16)
 
         def one(i, carry):
-            other = lax.rem(ep + i, ep_size)
-
-            @pl.when(lax.rem(other, CHUNKS) == ch)
+            other = bounds[ch] + lax.rem(ep + i, sources[ch])
+
+            @pl.when(other != ep)
             def _():
                 pltpu.make_async_remote_copy(
-                    src_ref=produced.at[block(place(other)), :],
+                    src_ref=produced.at[block(other), :],
                     dst_ref=returned.at[block(ep), :],
                     send_sem=ret_send,
                     recv_sem=ret_recv,
@@ -359,11 +394,11 @@
 
             return carry
 
-        lax.fori_loop(1, ep_size, one, 0)
-
-        @pl.when(lax.rem(ep, CHUNKS) == ch)
+        lax.fori_loop(0, sources[ch], one, 0)
+
+        @pl.when(inside(ep, ch))
         def _():
-            returned[block(ep), :] = produced[block(place(ep)), :]
+            returned[block(ep), :] = produced[block(ep), :]
 
     def first_rows():
         halo_copy.wait_recv()
@@ -375,21 +410,24 @@
         ).astype(jnp.bfloat16)
 
     streams = {"m": mix, "t": tok, "h": hdn}
+    weights = {"mc": [0], "tc": [1, 2], "hc": [3]}
     for entry in order:
         kind = entry[0]
+        for i in weights.pop(kind, ()):
+            w_copies[i].wait()
         if kind in streams:
             move(streams[kind], entry[1], entry[2])
         elif kind == "disp":
             lax.fori_loop(1, ep_size, dispatch, 0)
+        elif kind == "pool":
+            pool(entry[1])
         elif kind == "first":
             first_rows()
         elif kind == "got":
             dispatched(entry[1])
-        elif kind == "w":
-            w_copies[entry[1]].wait()
         elif kind == "mc":
-            mate_wait(mix, 0, entry[1])
-            for_origins(entry[1], mix_item(entry[1] == 0))
+            mate_wait(mix, entry[1], entry[2])
+            for_origins(entry[2], mix_item(entry[1], entry[2] == 0))
         elif kind == "mo":
             mixed_out[...] = acc_m[...].astype(jnp.bfloat16)
         elif kind == "tc":
@@ -397,7 +435,7 @@
             for_origins(entry[2], token_item(entry[1], entry[2] == 0))
         elif kind == "act":
             activate(entry[1])
-        elif kind == "dc":
+        elif kind == "hc":
             mate_wait(hdn, entry[1], entry[2])
             for_origins(entry[2], down_item(entry[1], entry[2] == 0))
         elif kind == "ret":
@@ -408,10 +446,10 @@
     pltpu.make_async_copy(outgoing.at[others, :], outgoing.at[others, :], disp_send).wait()
     pltpu.make_async_copy(produced.at[others, :], produced.at[others, :], ret_send).wait()
     for stream in streams.values():
-        for piece in range(stream.pieces):
-            ref = stream.buf.at[pl.ds(0, ny - 1), 0, pl.ds(0, stream.rows), :]
+        for piece in range(2 * len(stream.group_rows)):
+            ref = stream.buf.at[pl.ds(0, ny - 1), 0, pl.ds(*stream.rows(piece)), :]
             pltpu.make_async_copy(ref, ref, stream.send.at[piece]).wait()
-            ref = stream.buf.at[pl.ds(0, ny), 0, pl.ds(0, stream.rows), :]
+            ref = stream.buf.at[pl.ds(0, ny), 0, pl.ds(*stream.rows(piece)), :]
             pltpu.make_async_copy(ref, ref, stream.mate_send.at[piece]).wait()
 
     slot_lanes = lax.broadcasted_iota(jnp.int32, (tokens, slots), 1)
@@ -427,52 +465,43 @@
     rows_out[...] = rows.astype(jnp.bfloat16)
 
 
-def full_order(half):
-    m = [1, 2, 3, 0]
-    order = [("m", 1, 0), ("m", 2, 0), ("m", 3, 0), ("disp",), ("first",), ("m", 0, 0)]
-    for hop in (1, 2):
-        order += [("m", p, hop) for p in m if hop <= half]
-    order += [("got", 0), ("t", 0, 0), ("t", 1, 0)]
-    for hop in range(3, half + 1):
-        order += [("m", p, hop) for p in m]
-    order += [("w", 0), ("mc", 0)]
-    order += [("got", 1)]
-
-    def t(ch, hop):
-        return [("t", 2 * ch, hop), ("t", 2 * ch + 1, hop)]
-
-    def h(ch, hop):
-        return [("h", 2 * ch, hop), ("h", 2 * ch + 1, hop)]
-
-    late = [("mc", hop) for hop in range(1, half + 1)] + [("mo",)]
-    order += [("w", 1), ("w", 2)]
+SOURCES = (12, 12, 8)
+ORDER = (
+    ("disp",), ("pool", 2), ("pool", 1), ("pool", 3), ("m", 1, 0), ("m", 3, 0), ("m", 2, 0),
+    ("pool", 0), ("first",), ("m", 0, 0), ("m", 1, 1), ("mc", 1, 0), ("m", 3, 1), ("m", 2, 1),
+    ("got", 0), ("t", 0, 0), ("m", 0, 1), ("got", 1), ("m", 1, 2), ("m", 3, 2), ("m", 2, 2),
+    ("t", 0, 1), ("m", 0, 2), ("t", 3, 0), ("got", 2), ("t", 5, 0), ("m", 3, 3), ("mc", 1, 1),
+    ("m", 2, 3), ("mc", 0, 0), ("t", 1, 0), ("t", 0, 2), ("t", 2, 0), ("tc", 0, 0), ("t", 4, 0),
+    ("t", 5, 1), ("t", 1, 1), ("m", 0, 3), ("tc", 2, 0), ("tc", 1, 0), ("mc", 1, 3), ("m", 3, 4),
+    ("mc", 0, 2), ("m", 2, 4), ("m", 1, 3), ("t", 2, 1), ("t", 3, 1), ("t", 4, 1), ("t", 1, 2),
+    ("mc", 0, 1), ("mc", 1, 4), ("m", 0, 4), ("tc", 0, 1), ("tc", 1, 1), ("t", 2, 2), ("t", 3, 2),
+    ("mc", 0, 3), ("t", 5, 2), ("t", 0, 3), ("t", 1, 3), ("t", 4, 2), ("m", 1, 4), ("mc", 0, 4),
+    ("t", 3, 3), ("t", 2, 3), ("tc", 0, 2), ("tc", 0, 3), ("tc", 2, 1), ("tc", 1, 2), ("t", 5, 3),
+    ("t", 1, 4), ("t", 0, 4), ("mc", 1, 2), ("t", 4, 3), ("tc", 1, 3), ("tc", 0, 4), ("act", 0),
+    ("h", 0, 0), ("h", 1, 0), ("t", 3, 4), ("t", 2, 4), ("t", 5, 4), ("tc", 2, 2), ("tc", 1, 4),
+    ("act", 1), ("h", 2, 0), ("t", 4, 4), ("tc", 2, 3), ("h", 3, 0), ("hc", 0, 0), ("h", 0, 1),
+    ("tc", 2, 4), ("act", 2), ("h", 4, 0), ("h", 5, 0), ("hc", 1, 0), ("h", 1, 1), ("h", 2, 1),
+    ("hc", 0, 1), ("h", 3, 1), ("h", 0, 2), ("h", 4, 1), ("h", 5, 1), ("h", 1, 2), ("h", 2, 2),
+    ("mo",), ("h", 3, 2), ("h", 4, 2), ("h", 5, 2), ("h", 0, 3), ("hc", 1, 1), ("hc", 2, 0),
+    ("h", 1, 3), ("h", 2, 3), ("hc", 1, 2), ("h", 3, 3), ("h", 4, 3), ("h", 5, 3), ("hc", 0, 2),
+    ("hc", 2, 2), ("hc", 2, 1), ("h", 1, 4), ("h", 0, 4), ("hc", 0, 3), ("hc", 1, 3), ("h", 2, 4),
+    ("h", 3, 4), ("hc", 0, 4), ("ret", 0), ("h", 4, 4), ("h", 5, 4), ("hc", 2, 3), ("hc", 1, 4),
+    ("ret", 1), ("hc", 2, 4), ("ret", 2),
+)
+
+
+def full_order(ep_size, half):
+    sources = SOURCES if ep_size == sum(SOURCES) else (1, ep_size - 2, 1)
     if half == 4:
-        order += t(0, 1) + [("t", 2, 0), late[0], ("tc", 0, 0)]
-        order += t(0, 2) + [("t", 3, 0), late[1], ("tc", 0, 1)]
-        order += t(0, 3) + [("t", 2, 1), late[2], ("tc", 0, 2)]
-        order += t(0, 4) + [("t", 3, 1), ("tc", 0, 3), ("t", 2, 2), ("tc", 0, 4), ("act", 0)]
-        order += [("h", 0, 0), ("h", 1, 0), ("t", 3, 2), ("tc", 1, 0), ("h", 0, 1), ("t", 2, 3)]
-        order += [("h", 1, 1), ("t", 3, 3), late[3], late[4], ("tc", 1, 1), ("w", 3), ("dc", 0, 0)]
-        order += h(0, 2) + [("tc", 1, 2), ("dc", 0, 1)] + t(1, 4)
-        order += [("tc", 1, 3)] + h(0, 3) + [("tc", 1, 4), ("act", 1)]
-        order += h(1, 0) + [("dc", 0, 2)] + h(0, 4) + h(1, 1)
-        order += [("dc", 0, 3), ("dc", 0, 4), ("ret", 0)]
-        order += h(1, 2) + [("dc", 1, 0)] + h(1, 3) + [("dc", 1, 1)] + h(1, 4)
-        order += [("dc", 1, 2), ("dc", 1, 3), ("dc", 1, 4), ("ret", 1)]
-    else:
-        order += t(1, 0)
-        for ch in range(CHUNKS):
-            for hop in range(1, half + 1):
-                order += t(ch, hop)
-            order += [("tc", ch, hop) for hop in range(half + 1)] + [("act", ch)]
-        order += late + [("w", 3)]
-        for ch in range(CHUNKS):
-            order += h(ch, 0)
-        for ch in range(CHUNKS):
-            for hop in range(1, half + 1):
-                order += h(ch, hop)
-            order += [("dc", ch, hop) for hop in range(half + 1)] + [("ret", ch)]
-    return order
+        return sources, ORDER
+    order = [("disp",), ("pool", 1), ("pool", 2), ("pool", 3), ("pool", 0), ("first",)]
+    for kind, groups in (("m", MIX_GROUPS), ("t", 3), ("h", 3)):
+        for g in range(groups):
+            order += [("got", g)] if kind == "t" else []
+            order += [(kind, 2 * g + q, hop) for hop in range(half + 1) for q in range(2)]
+            order += [(kind + "c", g, hop) for hop in range(half + 1)]
+            order += {"m": [("mo",)] * (g == 1), "t": [("act", g)], "h": [("ret", g)]}[kind]
+    return sources, order
 
 
 def solution(mesh):
@@ -489,24 +518,33 @@
         vmem, dma = pltpu.VMEM, pltpu.SemaphoreType.DMA
         bf16, f32 = jnp.bfloat16, jnp.float32
 
-        def stream_sems(pieces, groups):
+        sources, order = full_order(ep_size, half)
+        chunks = len(sources)
+
+        def stream_sems(groups):
+            pieces = 2 * groups
             return [dma((pieces,)), dma((pieces, 2, half)), dma((pieces,)), dma((groups, half + 1))]
 
         here = pl.BlockSpec(memory_space=pltpu.VMEM)
-        there = pl.BlockSpec(memory_space=pl.ANY)
+        there = pl.BlockSpec(memory_space=pltpu.HBM)
         flops = 2 * (length * chans * tp_size * width + slots * (feats * tp_size * 2 * hid + hid * tp_size * width))
         call = pl.pallas_call(
             functools.partial(
-                kernel, ep_size, tp_size, chans * tp_size // 4, full_order(half)
+                kernel, ep_size, tp_size, chans * tp_size // 4, sources, order
             ),
             name="mixer_and_experts",
             out_shape=(
                 jax.ShapeDtypeStruct((length, width), bf16),
                 jax.ShapeDtypeStruct((tokens, width), bf16),
             ),
-            in_specs=[here] * 5 + [there] * 4,
+            in_specs=[there] * 9,
             out_specs=(here, here),
             scratch_shapes=[
+                vmem((length, chans), bf16),
+                vmem((tokens, feats), bf16),
+                vmem((TOP, tokens), jnp.int32),
+                vmem((TOP, tokens), f32),
+                vmem((1, feats * tp_size), f32),
                 vmem(mix_weight.shape, bf16),
                 vmem((feats * tp_size, 2 * hid), bf16),
                 vmem(down_weight.shape[1:], bf16),
@@ -523,22 +561,23 @@
                 vmem((slots, width), f32),
                 vmem((slots, 128), f32),
                 vmem((tokens, tokens), f32),
+                dma((5,)),
                 dma((4,)),
                 dma((2,)),
                 dma,
-                dma((CHUNKS,)),
+                dma((chunks,)),
                 dma,
                 dma,
             ]
-            + stream_sems(MIX_PIECES, 1)
-            + stream_sems(2 * CHUNKS, CHUNKS)
-            + stream_sems(2 * CHUNKS, CHUNKS),
+            + stream_sems(MIX_GROUPS)
+            + stream_sems(chunks)
+            + stream_sems(chunks),
             compiler_params=pltpu.CompilerParams(
-                collective_id=0, has_side_effects=True, vmem_limit_bytes=60 * 1024 * 1024
+                collective_id=0, has_side_effects=True, vmem_limit_bytes=24 * 1024 * 1024
             ),
             cost_estimate=pl.CostEstimate(flops=flops, bytes_accessed=8 * 1024 * 1024, transcendentals=0),
         )
-        return call(
+        operands = (
             mix_input,
             expert_input,
             expert_index.T,
@@ -549,6 +588,7 @@
             up_weight[0],
             down_weight[0],
         )
+        return call(*(pltpu.with_memory_space_constraint(a, pltpu.HBM) for a in operands))
 
     placed = (
         P("ep", "tp"),

time: 89 us -> 80.5 us (0.904)
  the two profiles are of different devices: /device:TPU:14 before, /device:TPU:1 now
where the time goes in v2:
time: 80.5 us; the launch traced here: 80.4 us
  Pallas kernels  78.4 us (97%)
  local copies, waits for them, and re-layouts  1.33 us (2%)
    pallas_call x1, Pallas kernels, shards(): call(*(pltpu.with_memory_space_constraint(a, pltpu.HBM) for a in operands))  78.4 us

profile of v2, /device:TPU:1, one launch (start us, length us, event | category | flops | bytes accessed | tf_op | source)
XLA Modules:
  0.0 80.4 jit_solution(14791968747063087649)
XLA Ops:
  0.6 78.4 %mixer_and_experts.1 = (bf16[512,256]{1,0:T(8,128)(2,1)S(1)}, bf16[128,256]{1,0:T(8,128)(2,1)S(1)}) custom-call(bf16[512,128]{1,0:T(8,128)(2,1)} %mix_hbm.1, bf16[128,256]{1,0:T(8,128)(2,1)} %x_hbm.1, s32[2,128]{1,0:T(2,128)} %bitcast.10, f32[2,128]{1,0:T(2,128)} %bitcast.11, f32[1,4096]{1,0:T(1,128)} %bitcast.9, bf16[2048,256]{1,0:T(8,128)(2,1)} %mix_w.1, ...), custom_call_target="tpu_custom_call" | custom-call | flops 2147483648 | bytes 8388608 | tf_op jit(solution)/shard_map/mixer_and_experts/pallas_call | solution.py:591
  79.1 0.7 copy.13
  79.8 0.6 copy.14

commit v3 on v2

--- a/solution.py
+++ b/solution.py
@@ -12,6 +12,8 @@
 REACH = 16
 EPS = 1e-06
 MIX_GROUPS = 2
+PARTS = ((0, 1), (2, 3), (4,))
+NX = 4
 
 
 class Stream:
@@ -27,6 +29,14 @@
     def rows(self, piece):
         size = self.group_rows[piece // 2] // 2
         return self.group_first[piece // 2] + (piece % 2) * size, size
+
+
+def far_first(nz, nx):
+    def hops(offset):
+        return min(offset[0], nz - offset[0]) + min(offset[1], nx - offset[1])
+
+    offsets = [(z, x) for z in range(nz) for x in range(nx) if z or x]
+    return sorted(offsets, key=lambda offset: (-hops(offset), offset))
 
 
 def kernel(
@@ -67,6 +77,7 @@
     acc_d,
     squares,
     columns,
+    takes,
     in_sem,
     w_sem,
     halo_sem,
@@ -100,6 +111,7 @@
     length, chans = mix_in.shape
     slots = outgoing.shape[0]
     cap = slots // ep_size
+    nx = NX if ep_size % NX == 0 else 1
     hid = hg.shape[3]
     chunks = [n * cap for n in sources]
     bounds = [sum(sources[:ch]) for ch in range(len(sources) + 1)]
@@ -219,20 +231,26 @@
     for bound in bounds[1:-1]:
         my_chunk = my_chunk + jnp.where(ep >= bound, 1, 0)
 
-    def dispatch(i, carry):
-        other = lax.rem(ep + i, ep_size)
-        pltpu.make_async_remote_copy(
-            src_ref=outgoing.at[block(other), :],
-            dst_ref=tg.at[y, core, block(ep), :],
-            send_sem=disp_send,
-            recv_sem=disp_recv.at[my_chunk],
-            device_id=(other, tp),
-            device_id_type=MESH,
-        ).start()
-        return carry
+    def dispatch():
+        for away_z, away_x in far_first(ep_size // nx, nx):
+            other = lax.rem(ep // nx + away_z, ep_size // nx) * nx + lax.rem(ep + away_x, nx)
+            pltpu.make_async_remote_copy(
+                src_ref=outgoing.at[block(other), :],
+                dst_ref=tg.at[y, core, block(ep), :],
+                send_sem=disp_send,
+                recv_sem=disp_recv.at[my_chunk],
+                device_id=(other, tp),
+                device_id_type=MESH,
+            ).start()
 
     def limit(piece, way):
         return half if (piece % 2 == 0) == (way == 0) else half - 1
+
+    def arrival(piece, way, hop):
+        return piece * (ny - 1) + way * limit(piece, 0) + hop - 1
+
+    def part_of(hop):
+        return [hop in hops for hops in PARTS].index(True)
 
     def part(stream, origin, piece):
         return stream.buf.at[origin, core, pl.ds(*stream.rows(piece)), :]
@@ -242,8 +260,8 @@
         pltpu.make_async_remote_copy(
             src_ref=ref,
             dst_ref=ref,
-            send_sem=stream.send.at[piece],
-            recv_sem=stream.recv.at[piece, way, hop],
+            send_sem=stream.send,
+            recv_sem=stream.recv.at[arrival(piece, way, hop + 1)],
             device_id=(ep, up if way == 0 else down),
             device_id_type=MESH,
         ).start()
@@ -253,8 +271,8 @@
         pltpu.make_async_remote_copy(
             src_ref=ref,
             dst_ref=ref,
-            send_sem=stream.mate_send.at[piece],
-            recv_sem=stream.mate_recv.at[piece // 2, hop],
+            send_sem=stream.mate_send,
+            recv_sem=stream.mate_recv.at[piece // 2, part_of(hop)],
             device_id=(ep, mate),
             device_id_type=MESH,
         ).start()
@@ -274,18 +292,20 @@
                 continue
             origin = origin_of(way, hop)
             ref = part(stream, origin, piece)
-            pltpu.make_async_copy(ref, ref, stream.recv.at[piece, way, hop - 1]).wait()
+            pltpu.make_async_copy(ref, ref, stream.recv.at[arrival(piece, way, hop)]).wait()
             if hop < limit(piece, way):
                 ring_send(stream, piece, way, origin, hop)
             mate_copy(stream, piece, origin, hop)
 
-    def mate_wait(stream, group_no, hop):
-        rows = stream.group_rows[group_no]
-        if 0 < hop < half:
-            ref = stream.buf.at[pl.ds(0, 2), 0, pl.ds(0, rows), :]
-        else:
-            ref = stream.buf.at[0, 0, pl.ds(0, rows), :]
-        pltpu.make_async_copy(ref, ref, stream.mate_recv.at[group_no, hop]).wait()
+    def mate_wait(stream, group_no, part_no):
+        origins = sum(1 if hop in (0, half) else 2 for hop in PARTS[part_no])
+        ref = stream.buf.at[pl.ds(0, origins), 0, stream.group(group_no), :]
+        pltpu.make_async_copy(ref, ref, stream.mate_recv.at[group_no, part_no]).wait()
+
+    def gathered(stream, group_no, part_no, item_of):
+        mate_wait(stream, group_no, part_no)
+        for hop in PARTS[part_no]:
+            for_origins(hop, item_of(group_no, hop == 0))
 
     def for_origins(hop, item):
         if hop == 0:
@@ -400,6 +420,11 @@
         def _():
             returned[block(ep), :] = produced[block(ep), :]
 
+    def find_takes():
+        slot_lanes = lax.broadcasted_iota(jnp.int32, (tokens, slots), 1)
+        for k in range(TOP):
+            takes[k] = (columns[:, k : k + 1].astype(jnp.int32) == slot_lanes).astype(jnp.bfloat16)
+
     def first_rows():
         halo_copy.wait_recv()
         ext[pl.ds(0, REACH), :] = jnp.where(ep == 0, 0.0, halo[...].astype(jnp.float32))
@@ -418,7 +443,9 @@
         if kind in streams:
             move(streams[kind], entry[1], entry[2])
         elif kind == "disp":
-            lax.fori_loop(1, ep_size, dispatch, 0)
+            dispatch()
+        elif kind == "take":
+            find_takes()
         elif kind == "pool":
             pool(entry[1])
         elif kind == "first":
@@ -426,18 +453,15 @@
         elif kind == "got":
             dispatched(entry[1])
         elif kind == "mc":
-            mate_wait(mix, entry[1], entry[2])
-            for_origins(entry[2], mix_item(entry[1], entry[2] == 0))
+            gathered(mix, entry[1], entry[2], mix_item)
         elif kind == "mo":
             mixed_out[...] = acc_m[...].astype(jnp.bfloat16)
         elif kind == "tc":
-            mate_wait(tok, entry[1], entry[2])
-            for_origins(entry[2], token_item(entry[1], entry[2] == 0))
+            gathered(tok, entry[1], entry[2], token_item)
         elif kind == "act":
             activate(entry[1])
         elif kind == "hc":
-            mate_wait(hdn, entry[1], entry[2])
-            for_origins(entry[2], down_item(entry[1], entry[2] == 0))
+            gathered(hdn, entry[1], entry[2], down_item)
         elif kind == "ret":
             give_back(entry[1])
 
@@ -446,17 +470,11 @@
     pltpu.make_async_copy(outgoing.at[others, :], outgoing.at[others, :], disp_send).wait()
     pltpu.make_async_copy(produced.at[others, :], produced.at[others, :], ret_send).wait()
     for stream in streams.values():
-        for piece in range(2 * len(stream.group_rows)):
-            ref = stream.buf.at[pl.ds(0, ny - 1), 0, pl.ds(*stream.rows(piece)), :]
-            pltpu.make_async_copy(ref, ref, stream.send.at[piece]).wait()
-            ref = stream.buf.at[pl.ds(0, ny), 0, pl.ds(*stream.rows(piece)), :]
-            pltpu.make_async_copy(ref, ref, stream.mate_send.at[piece]).wait()
-
-    slot_lanes = lax.broadcasted_iota(jnp.int32, (tokens, slots), 1)
-    takes = [
-        (columns[:, k : k + 1].astype(jnp.int32) == slot_lanes).astype(jnp.bfloat16)
-        for k in range(TOP)
-    ]
+        ref = stream.buf.at[pl.ds(0, ny - 1), 0, :, :]
+        pltpu.make_async_copy(ref, ref, stream.send).wait()
+        ref = stream.buf.at[:, 0, :, :]
+        pltpu.make_async_copy(ref, ref, stream.mate_send).wait()
+
     pltpu.make_async_copy(returned.at[others, :], returned.at[others, :], ret_recv).wait()
     rows = 0.0
     for k in range(TOP):
@@ -465,43 +483,31 @@
     rows_out[...] = rows.astype(jnp.bfloat16)
 
 
-SOURCES = (12, 12, 8)
+SOURCES = (8, 8, 8, 8)
 ORDER = (
-    ("disp",), ("pool", 2), ("pool", 1), ("pool", 3), ("m", 1, 0), ("m", 3, 0), ("m", 2, 0),
-    ("pool", 0), ("first",), ("m", 0, 0), ("m", 1, 1), ("mc", 1, 0), ("m", 3, 1), ("m", 2, 1),
-    ("got", 0), ("t", 0, 0), ("m", 0, 1), ("got", 1), ("m", 1, 2), ("m", 3, 2), ("m", 2, 2),
-    ("t", 0, 1), ("m", 0, 2), ("t", 3, 0), ("got", 2), ("t", 5, 0), ("m", 3, 3), ("mc", 1, 1),
-    ("m", 2, 3), ("mc", 0, 0), ("t", 1, 0), ("t", 0, 2), ("t", 2, 0), ("tc", 0, 0), ("t", 4, 0),
-    ("t", 5, 1), ("t", 1, 1), ("m", 0, 3), ("tc", 2, 0), ("tc", 1, 0), ("mc", 1, 3), ("m", 3, 4),
-    ("mc", 0, 2), ("m", 2, 4), ("m", 1, 3), ("t", 2, 1), ("t", 3, 1), ("t", 4, 1), ("t", 1, 2),
-    ("mc", 0, 1), ("mc", 1, 4), ("m", 0, 4), ("tc", 0, 1), ("tc", 1, 1), ("t", 2, 2), ("t", 3, 2),
-    ("mc", 0, 3), ("t", 5, 2), ("t", 0, 3), ("t", 1, 3), ("t", 4, 2), ("m", 1, 4), ("mc", 0, 4),
-    ("t", 3, 3), ("t", 2, 3), ("tc", 0, 2), ("tc", 0, 3), ("tc", 2, 1), ("tc", 1, 2), ("t", 5, 3),
-    ("t", 1, 4), ("t", 0, 4), ("mc", 1, 2), ("t", 4, 3), ("tc", 1, 3), ("tc", 0, 4), ("act", 0),
-    ("h", 0, 0), ("h", 1, 0), ("t", 3, 4), ("t", 2, 4), ("t", 5, 4), ("tc", 2, 2), ("tc", 1, 4),
-    ("act", 1), ("h", 2, 0), ("t", 4, 4), ("tc", 2, 3), ("h", 3, 0), ("hc", 0, 0), ("h", 0, 1),
-    ("tc", 2, 4), ("act", 2), ("h", 4, 0), ("h", 5, 0), ("hc", 1, 0), ("h", 1, 1), ("h", 2, 1),
-    ("hc", 0, 1), ("h", 3, 1), ("h", 0, 2), ("h", 4, 1), ("h", 5, 1), ("h", 1, 2), ("h", 2, 2),
-    ("mo",), ("h", 3, 2), ("h", 4, 2), ("h", 5, 2), ("h", 0, 3), ("hc", 1, 1), ("hc", 2, 0),
-    ("h", 1, 3), ("h", 2, 3), ("hc", 1, 2), ("h", 3, 3), ("h", 4, 3), ("h", 5, 3), ("hc", 0, 2),
-    ("hc", 2, 2), ("hc", 2, 1), ("h", 1, 4), ("h", 0, 4), ("hc", 0, 3), ("hc", 1, 3), ("h", 2, 4),
-    ("h", 3, 4), ("hc", 0, 4), ("ret", 0), ("h", 4, 4), ("h", 5, 4), ("hc", 2, 3), ("hc", 1, 4),
-    ("ret", 1), ("hc", 2, 4), ("ret", 2),
+    ("disp",), ("pool", 1), ("pool", 2), ("pool", 3), ("m", 1, 0), ("m", 2, 0), ("m", 2, 1),
+    ("take",), ("got", 1), ("got", 3), ("got", 2), ("t", 7, 0), ("got", 0), ("t", 0, 0),
+    ("t", 1, 0), ("t", 6, 0), ("t", 3, 0), ("t", 5, 0), ("t", 4, 0), ("t", 2, 0), ("t", 0, 1),
+    ("t", 1, 1), ("pool", 0), ("first",), ("t", 3, 1), ("t", 5, 1), ("t", 7, 1), ("t", 2, 1),
+    ("t", 4, 1), ("t", 0, 2), ("t", 1, 2), ("t", 6, 1), ("t", 3, 2), ("tc", 3, 0), ("t", 2, 2),
+    ("t", 5, 2), ("t", 4, 2), ("t", 1, 3), ("tc", 1, 0), ("t", 0, 3), ("tc", 0, 0), ("t", 6, 2),
+    ("t", 7, 2), ("t", 3, 3), ("t", 2, 3), ("t", 5, 3), ("m", 3, 0), ("t", 4, 3), ("m", 1, 1),
+    ("t", 1, 4), ("t", 0, 4), ("tc", 0, 1), ("t", 6, 3), ("tc", 2, 0), ("t", 7, 3), ("tc", 0, 2),
+    ("act", 0), ("h", 0, 0), ("m", 0, 0), ("h", 1, 0), ("t", 3, 4), ("t", 2, 4), ("tc", 1, 1),
+    ("t", 5, 4), ("m", 2, 2), ("tc", 3, 1), ("tc", 1, 2), ("t", 4, 4), ("act", 1), ("h", 2, 0),
+    ("m", 1, 2), ("h", 3, 0), ("tc", 2, 1), ("t", 7, 4), ("t", 6, 4), ("h", 0, 1), ("tc", 2, 2),
+    ("act", 2), ("h", 5, 0), ("h", 4, 0), ("h", 1, 1), ("tc", 3, 2), ("act", 3), ("h", 7, 0),
+    ("h", 6, 0), ("h", 2, 1), ("m", 3, 1), ("h", 0, 2), ("h", 5, 1), ("h", 4, 1), ("h", 3, 1),
+    ("h", 1, 2), ("h", 7, 1), ("h", 6, 1), ("h", 2, 2), ("hc", 0, 0), ("hc", 1, 0), ("m", 0, 1),
+    ("hc", 2, 0), ("h", 5, 2), ("h", 4, 2), ("h", 3, 2), ("h", 0, 3), ("h", 1, 3), ("h", 7, 2),
+    ("h", 6, 2), ("h", 2, 3), ("m", 3, 2), ("mc", 1, 0), ("hc", 0, 1), ("h", 5, 3), ("h", 4, 3),
+    ("m", 0, 2), ("h", 3, 3), ("h", 1, 4), ("h", 7, 3), ("h", 0, 4), ("h", 6, 3), ("hc", 3, 0),
+    ("hc", 2, 1), ("m", 2, 3), ("m", 1, 3), ("hc", 0, 2), ("ret", 0), ("h", 2, 4), ("h", 5, 4),
+    ("h", 4, 4), ("m", 3, 3), ("hc", 1, 1), ("m", 0, 3), ("h", 3, 4), ("h", 7, 4), ("h", 6, 4),
+    ("hc", 2, 2), ("ret", 2), ("hc", 3, 1), ("hc", 1, 2), ("ret", 1), ("m", 1, 4), ("hc", 3, 2),
+    ("ret", 3), ("mc", 0, 0), ("mc", 1, 1), ("m", 2, 4), ("m", 0, 4), ("m", 3, 4), ("mc", 0, 1),
+    ("mc", 0, 2), ("mc", 1, 2), ("mo",),
 )
-
-
-def full_order(ep_size, half):
-    sources = SOURCES if ep_size == sum(SOURCES) else (1, ep_size - 2, 1)
-    if half == 4:
-        return sources, ORDER
-    order = [("disp",), ("pool", 1), ("pool", 2), ("pool", 3), ("pool", 0), ("first",)]
-    for kind, groups in (("m", MIX_GROUPS), ("t", 3), ("h", 3)):
-        for g in range(groups):
-            order += [("got", g)] if kind == "t" else []
-            order += [(kind, 2 * g + q, hop) for hop in range(half + 1) for q in range(2)]
-            order += [(kind + "c", g, hop) for hop in range(half + 1)]
-            order += {"m": [("mo",)] * (g == 1), "t": [("act", g)], "h": [("ret", g)]}[kind]
-    return sources, order
 
 
 def solution(mesh):
@@ -518,19 +524,18 @@
         vmem, dma = pltpu.VMEM, pltpu.SemaphoreType.DMA
         bf16, f32 = jnp.bfloat16, jnp.float32
 
-        sources, order = full_order(ep_size, half)
+        sources = SOURCES if ep_size == sum(SOURCES) else (ep_size // len(SOURCES),) * len(SOURCES)
         chunks = len(sources)
 
         def stream_sems(groups):
-            pieces = 2 * groups
-            return [dma((pieces,)), dma((pieces, 2, half)), dma((pieces,)), dma((groups, half + 1))]
+            return [dma, dma((2 * groups * (ny - 1),)), dma, dma((groups, len(PARTS)))]
 
         here = pl.BlockSpec(memory_space=pltpu.VMEM)
         there = pl.BlockSpec(memory_space=pltpu.HBM)
         flops = 2 * (length * chans * tp_size * width + slots * (feats * tp_size * 2 * hid + hid * tp_size * width))
         call = pl.pallas_call(
             functools.partial(
-                kernel, ep_size, tp_size, chans * tp_size // 4, sources, order
+                kernel, ep_size, tp_size, chans * tp_size // 4, sources, ORDER
             ),
             name="mixer_and_experts",
             out_shape=(
@@ -561,6 +566,7 @@
                 vmem((slots, width), f32),
                 vmem((slots, 128), f32),
                 vmem((tokens, tokens), f32),
+                vmem((TOP, tokens, slots), bf16),
                 dma((5,)),
                 dma((4,)),
                 dma((2,)),

time: 80.5 us -> 73.4 us (0.912)
  Pallas kernels: 78.4 us -> 70.7 us
    pallas_call x1, Pallas kernels: 78.4 us -> 70.7 us  [shards(): call(*(pltpu.with_memory_space_constraint(a, pltpu.HBM) for a in operands))]
where the time goes in v3:
time: 73.4 us; the launch traced here: 72.6 us
  Pallas kernels  70.7 us (96%)
  local copies, waits for them, and re-layouts  1.33 us (2%)
    pallas_call x1, Pallas kernels, shards(): call(*(pltpu.with_memory_space_constraint(a, pltpu.HBM) for a in operands))  70.7 us

profile of v3, /device:TPU:1, one launch (start us, length us, event | category | flops | bytes accessed | tf_op | source)
XLA Modules:
  0.0 72.6 jit_solution(17281189842626617201)
XLA Ops:
  0.6 70.7 %mixer_and_experts.1 = (bf16[512,256]{1,0:T(8,128)(2,1)S(1)}, bf16[128,256]{1,0:T(8,128)(2,1)S(1)}) custom-call(bf16[512,128]{1,0:T(8,128)(2,1)} %mix_hbm.1, bf16[128,256]{1,0:T(8,128)(2,1)} %x_hbm.1, s32[2,128]{1,0:T(2,128)} %bitcast.10, f32[2,128]{1,0:T(2,128)} %bitcast.11, f32[1,4096]{1,0:T(1,128)} %bitcast.9, bf16[2048,256]{1,0:T(8,128)(2,1)} %mix_w.1, ...), custom_call_target="tpu_custom_call" | custom-call | flops 2147483648 | bytes 8388608 | tf_op jit(solution)/shard_map/mixer_and_experts/pallas_call | solution.py:597
  71.3 0.7 copy.13
  72.0 0.6 copy.14

commit v4 on v3

--- a/solution.py
+++ b/solution.py
@@ -14,6 +14,7 @@
 MIX_GROUPS = 2
 PARTS = ((0, 1), (2, 3), (4,))
 NX = 4
+HALVES = 1
 
 
 class Stream:
@@ -113,15 +114,28 @@
     cap = slots // ep_size
     nx = NX if ep_size % NX == 0 else 1
     hid = hg.shape[3]
-    chunks = [n * cap for n in sources]
-    bounds = [sum(sources[:ch]) for ch in range(len(sources) + 1)]
+    part = cap // HALVES
+    sets = len(sources)
+    bounds = [sum(sources[:g]) for g in range(sets + 1)]
+    chunks = [sources[ch // HALVES] * part for ch in range(sets * HALVES)]
 
     mix = Stream(pg, [length // MIX_GROUPS] * MIX_GROUPS, (m_send, m_recv, m_mate_send, m_mate_recv))
     tok = Stream(tg, chunks, (t_send, t_recv, t_mate_send, t_mate_recv))
     hdn = Stream(hg, chunks, (h_send, h_recv, h_mate_send, h_mate_recv))
 
-    def block(i):
-        return pl.ds(pl.multiple_of(i * cap, cap), cap)
+    def sent_block(half_no, expert):
+        return pl.ds(pl.multiple_of((half_no * ep_size + expert) * part, part), part)
+
+    def chunk_block(ch, source):
+        first = sum(chunks[:ch])
+        return pl.ds(pl.multiple_of(first + (source - bounds[ch // HALVES]) * part, part), part)
+
+    def my_block(half_no):
+        first = (bounds[0] * HALVES + half_no * sources[0] + ep - bounds[0]) * part
+        for g in range(1, sets):
+            at = (bounds[g] * HALVES + half_no * sources[g] + ep - bounds[g]) * part
+            first = jnp.where(ep >= bounds[g], at, first)
+        return pl.ds(pl.multiple_of(first, part), part)
 
     in_copies = [
         pltpu.make_async_copy(src, dst, in_sem.at[i])
@@ -175,7 +189,11 @@
         jnp.sum(earlier * hits[0], axis=0, keepdims=True),
         jnp.sum((earlier + hits[0]) * hits[1], axis=0, keepdims=True),
     ]
-    targets = [named[k] * cap + ranks[k].astype(jnp.int32) for k in range(TOP)]
+    targets = []
+    for k in range(TOP):
+        rank = ranks[k].astype(jnp.int32)
+        half_no = sum((rank >= part * i).astype(jnp.int32) for i in range(1, HALVES))
+        targets.append((half_no * ep_size + named[k] - half_no) * part + rank)
     slot_rows = lax.broadcasted_iota(jnp.int32, (slots, tokens), 0)
     picks = jnp.logical_or(slot_rows == targets[0], slot_rows == targets[1])
     outgoing[...] = jnp.dot(
@@ -227,21 +245,22 @@
     )
     halo_copy.start()
 
-    my_chunk = 0
+    my_set = 0
     for bound in bounds[1:-1]:
-        my_chunk = my_chunk + jnp.where(ep >= bound, 1, 0)
+        my_set = my_set + jnp.where(ep >= bound, 1, 0)
 
     def dispatch():
-        for away_z, away_x in far_first(ep_size // nx, nx):
-            other = lax.rem(ep // nx + away_z, ep_size // nx) * nx + lax.rem(ep + away_x, nx)
-            pltpu.make_async_remote_copy(
-                src_ref=outgoing.at[block(other), :],
-                dst_ref=tg.at[y, core, block(ep), :],
-                send_sem=disp_send,
-                recv_sem=disp_recv.at[my_chunk],
-                device_id=(other, tp),
-                device_id_type=MESH,
-            ).start()
+        for half_no in range(HALVES):
+            for away_z, away_x in far_first(ep_size // nx, nx):
+                other = lax.rem(ep // nx + away_z, ep_size // nx) * nx + lax.rem(ep + away_x, nx)
+                pltpu.make_async_remote_copy(
+                    src_ref=outgoing.at[sent_block(half_no, other), :],
+                    dst_ref=tg.at[y, core, my_block(half_no), :],
+                    send_sem=disp_send,
+                    recv_sem=disp_recv.at[my_set * HALVES + half_no],
+                    device_id=(other, tp),
+                    device_id_type=MESH,
+                ).start()
 
     def limit(piece, way):
         return half if (piece % 2 == 0) == (way == 0) else half - 1
@@ -252,11 +271,11 @@
     def part_of(hop):
         return [hop in hops for hops in PARTS].index(True)
 
-    def part(stream, origin, piece):
+    def piece_of(stream, origin, piece):
         return stream.buf.at[origin, core, pl.ds(*stream.rows(piece)), :]
 
     def ring_send(stream, piece, way, origin, hop):
-        ref = part(stream, origin, piece)
+        ref = piece_of(stream, origin, piece)
         pltpu.make_async_remote_copy(
             src_ref=ref,
             dst_ref=ref,
@@ -267,7 +286,7 @@
         ).start()
 
     def mate_copy(stream, piece, origin, hop):
-        ref = part(stream, origin, piece)
+        ref = piece_of(stream, origin, piece)
         pltpu.make_async_remote_copy(
             src_ref=ref,
             dst_ref=ref,
@@ -291,7 +310,7 @@
             if hop > limit(piece, way):
                 continue
             origin = origin_of(way, hop)
-            ref = part(stream, origin, piece)
+            ref = piece_of(stream, origin, piece)
             pltpu.make_async_copy(ref, ref, stream.recv.at[arrival(piece, way, hop)]).wait()
             if hop < limit(piece, way):
                 ring_send(stream, piece, way, origin, hop)
@@ -302,70 +321,48 @@
         ref = stream.buf.at[pl.ds(0, origins), 0, stream.group(group_no), :]
         pltpu.make_async_copy(ref, ref, stream.mate_recv.at[group_no, part_no]).wait()
 
-    def gathered(stream, group_no, part_no, item_of):
+    def origins_of(part_no):
+        found = []
+        for hop in PARTS[part_no]:
+            found += [y] if hop == 0 else [origin_of(0, hop)]
+            found += [origin_of(1, hop)] if 0 < hop < half else []
+        return found
+
+    def gathered(stream, group_no, part_no, totals, term):
         mate_wait(stream, group_no, part_no)
-        for hop in PARTS[part_no]:
-            for_origins(hop, item_of(group_no, hop == 0))
-
-    def for_origins(hop, item):
-        if hop == 0:
-            item(y)
-        elif hop == half:
-            item(origin_of(0, hop))
-        else:
-
-            def both(way, carry):
-                item(lax.rem(y + ny + (2 * way - 1) * hop, ny))
-                return carry
-
-            lax.fori_loop(0, 2, both, 0)
-
-    def mix_item(g, first):
-        at = mix.group(g)
-
-        def item(origin):
-            a = jnp.concatenate([pg[origin, 0, at, :], pg[origin, 1, at, :]], axis=1)
-            rows = pl.ds(pl.multiple_of(origin * 2 * chans, 2 * chans), 2 * chans)
-            got = jnp.dot(a, mw[rows, :], preferred_element_type=jnp.float32)
-            acc_m[at, :] = got if first else acc_m[at, :] + got
-
-        return item
-
-    def token_item(ch, first):
-        at = tok.group(ch)
-
-        def item(origin):
-            scaled, sums = [], 0.0
-            for j in range(2):
-                x = tg[origin, j, at, :].astype(jnp.float32)
-                lanes = pl.ds(pl.multiple_of((origin * 2 + j) * feats, feats), feats)
-                scaled.append((x * gain_in[:, lanes]).astype(jnp.bfloat16))
-                sq = x * x
-                for q in range(0, feats, 128):
-                    sums = sums + sq[:, q : q + 128]
-            rows = pl.ds(pl.multiple_of(origin * 2 * feats, 2 * feats), 2 * feats)
-            got = jnp.dot(
-                jnp.concatenate(scaled, axis=1), wgu[rows, :], preferred_element_type=jnp.float32
-            )
-            if first:
-                acc_t[at, :] = got
-                squares[at, :] = sums
-            else:
-                acc_t[at, :] = acc_t[at, :] + got
-                squares[at, :] = squares[at, :] + sums
-
-        return item
-
-    def down_item(ch, first):
-        at = tok.group(ch)
-
-        def item(origin):
-            a = jnp.concatenate([hg[origin, 0, at, :], hg[origin, 1, at, :]], axis=1)
-            rows = pl.ds(pl.multiple_of(origin * 2 * hid, 2 * hid), 2 * hid)
-            got = jnp.dot(a, wd[rows, :], preferred_element_type=jnp.float32)
-            acc_d[at, :] = got if first else acc_d[at, :] + got
-
-        return item
+        at = stream.group(group_no)
+        sums = [0.0] * len(totals)
+        for origin in origins_of(part_no):
+            sums = [a + b for a, b in zip(sums, term(origin, at))]
+        for total, value in zip(totals, sums):
+            total[at, :] = value if part_no == 0 else total[at, :] + value
+
+    def rows_of(origin, size):
+        return pl.ds(pl.multiple_of(origin * size, size), size)
+
+    def mix_term(origin, at):
+        a = jnp.concatenate([pg[origin, 0, at, :], pg[origin, 1, at, :]], axis=1)
+        return [jnp.dot(a, mw[rows_of(origin, 2 * chans), :], preferred_element_type=jnp.float32)]
+
+    def token_term(origin, at):
+        scaled, sums = [], 0.0
+        for j in range(2):
+            x = tg[origin, j, at, :].astype(jnp.float32)
+            lanes = pl.ds(pl.multiple_of((origin * 2 + j) * feats, feats), feats)
+            scaled.append((x * gain_in[:, lanes]).astype(jnp.bfloat16))
+            sq = x * x
+            for q in range(0, feats, 128):
+                sums = sums + sq[:, q : q + 128]
+        got = jnp.dot(
+            jnp.concatenate(scaled, axis=1),
+            wgu[rows_of(origin, 2 * feats), :],
+            preferred_element_type=jnp.float32,
+        )
+        return [got, sums]
+
+    def down_term(origin, at):
+        a = jnp.concatenate([hg[origin, 0, at, :], hg[origin, 1, at, :]], axis=1)
+        return [jnp.dot(a, wd[rows_of(origin, 2 * hid), :], preferred_element_type=jnp.float32)]
 
     def activate(ch):
         at = tok.group(ch)
@@ -376,7 +373,8 @@
         hg[y, core, at, :] = (gate / (1.0 + jnp.exp(-gate)) * upper).astype(jnp.bfloat16)
 
     def inside(device, ch):
-        return jnp.logical_and(device >= bounds[ch], device < bounds[ch + 1])
+        g = ch // HALVES
+        return jnp.logical_and(device >= bounds[g], device < bounds[g + 1])
 
     def dispatched(ch):
         base, rows = tok.group_first[ch], chunks[ch]
@@ -384,10 +382,10 @@
 
         @pl.when(mine)
         def _():
-            if rows > cap:
-                ref = tg.at[0, 0, pl.ds(base, rows - cap), :]
+            if rows > part:
+                ref = tg.at[0, 0, pl.ds(base, rows - part), :]
                 pltpu.make_async_copy(ref, ref, disp_recv.at[ch]).wait()
-            tg[y, core, block(ep), :] = outgoing[block(ep), :]
+            tg[y, core, chunk_block(ch, ep), :] = outgoing[sent_block(ch % HALVES, ep), :]
 
         @pl.when(jnp.logical_not(mine))
         def _():
@@ -397,15 +395,16 @@
     def give_back(ch):
         at = tok.group(ch)
         produced[at, :] = acc_d[at, :].astype(jnp.bfloat16)
+        g, half_no = ch // HALVES, ch % HALVES
 
         def one(i, carry):
-            other = bounds[ch] + lax.rem(ep + i, sources[ch])
+            other = bounds[g] + lax.rem(ep + i, sources[g])
 
             @pl.when(other != ep)
             def _():
                 pltpu.make_async_remote_copy(
-                    src_ref=produced.at[block(other), :],
-                    dst_ref=returned.at[block(ep), :],
+                    src_ref=produced.at[chunk_block(ch, other), :],
+                    dst_ref=returned.at[sent_block(half_no, ep), :],
                     send_sem=ret_send,
                     recv_sem=ret_recv,
                     device_id=(other, tp),
@@ -414,11 +413,11 @@
 
             return carry
 
-        lax.fori_loop(0, sources[ch], one, 0)
+        lax.fori_loop(0, sources[g], one, 0)
 
         @pl.when(inside(ep, ch))
         def _():
-            returned[block(ep), :] = produced[block(ep), :]
+            returned[sent_block(half_no, ep), :] = produced[chunk_block(ch, ep), :]
 
     def find_takes():
         slot_lanes = lax.broadcasted_iota(jnp.int32, (tokens, slots), 1)
@@ -453,15 +452,15 @@
         elif kind == "got":
             dispatched(entry[1])
         elif kind == "mc":
-            gathered(mix, entry[1], entry[2], mix_item)
+            gathered(mix, entry[1], entry[2], [acc_m], mix_term)
         elif kind == "mo":
             mixed_out[...] = acc_m[...].astype(jnp.bfloat16)
         elif kind == "tc":
-            gathered(tok, entry[1], entry[2], token_item)
+            gathered(tok, entry[1], entry[2], [acc_t, squares], token_term)
         elif kind == "act":
             activate(entry[1])
         elif kind == "hc":
-            gathered(hdn, entry[1], entry[2], down_item)
+            gathered(hdn, entry[1], entry[2], [acc_d], down_term)
         elif kind == "ret":
             give_back(entry[1])
 
@@ -485,28 +484,28 @@
 
 SOURCES = (8, 8, 8, 8)
 ORDER = (
-    ("disp",), ("pool", 1), ("pool", 2), ("pool", 3), ("m", 1, 0), ("m", 2, 0), ("m", 2, 1),
-    ("take",), ("got", 1), ("got", 3), ("got", 2), ("t", 7, 0), ("got", 0), ("t", 0, 0),
-    ("t", 1, 0), ("t", 6, 0), ("t", 3, 0), ("t", 5, 0), ("t", 4, 0), ("t", 2, 0), ("t", 0, 1),
-    ("t", 1, 1), ("pool", 0), ("first",), ("t", 3, 1), ("t", 5, 1), ("t", 7, 1), ("t", 2, 1),
-    ("t", 4, 1), ("t", 0, 2), ("t", 1, 2), ("t", 6, 1), ("t", 3, 2), ("tc", 3, 0), ("t", 2, 2),
-    ("t", 5, 2), ("t", 4, 2), ("t", 1, 3), ("tc", 1, 0), ("t", 0, 3), ("tc", 0, 0), ("t", 6, 2),
-    ("t", 7, 2), ("t", 3, 3), ("t", 2, 3), ("t", 5, 3), ("m", 3, 0), ("t", 4, 3), ("m", 1, 1),
-    ("t", 1, 4), ("t", 0, 4), ("tc", 0, 1), ("t", 6, 3), ("tc", 2, 0), ("t", 7, 3), ("tc", 0, 2),
-    ("act", 0), ("h", 0, 0), ("m", 0, 0), ("h", 1, 0), ("t", 3, 4), ("t", 2, 4), ("tc", 1, 1),
-    ("t", 5, 4), ("m", 2, 2), ("tc", 3, 1), ("tc", 1, 2), ("t", 4, 4), ("act", 1), ("h", 2, 0),
-    ("m", 1, 2), ("h", 3, 0), ("tc", 2, 1), ("t", 7, 4), ("t", 6, 4), ("h", 0, 1), ("tc", 2, 2),
-    ("act", 2), ("h", 5, 0), ("h", 4, 0), ("h", 1, 1), ("tc", 3, 2), ("act", 3), ("h", 7, 0),
-    ("h", 6, 0), ("h", 2, 1), ("m", 3, 1), ("h", 0, 2), ("h", 5, 1), ("h", 4, 1), ("h", 3, 1),
-    ("h", 1, 2), ("h", 7, 1), ("h", 6, 1), ("h", 2, 2), ("hc", 0, 0), ("hc", 1, 0), ("m", 0, 1),
-    ("hc", 2, 0), ("h", 5, 2), ("h", 4, 2), ("h", 3, 2), ("h", 0, 3), ("h", 1, 3), ("h", 7, 2),
-    ("h", 6, 2), ("h", 2, 3), ("m", 3, 2), ("mc", 1, 0), ("hc", 0, 1), ("h", 5, 3), ("h", 4, 3),
-    ("m", 0, 2), ("h", 3, 3), ("h", 1, 4), ("h", 7, 3), ("h", 0, 4), ("h", 6, 3), ("hc", 3, 0),
-    ("hc", 2, 1), ("m", 2, 3), ("m", 1, 3), ("hc", 0, 2), ("ret", 0), ("h", 2, 4), ("h", 5, 4),
-    ("h", 4, 4), ("m", 3, 3), ("hc", 1, 1), ("m", 0, 3), ("h", 3, 4), ("h", 7, 4), ("h", 6, 4),
-    ("hc", 2, 2), ("ret", 2), ("hc", 3, 1), ("hc", 1, 2), ("ret", 1), ("m", 1, 4), ("hc", 3, 2),
-    ("ret", 3), ("mc", 0, 0), ("mc", 1, 1), ("m", 2, 4), ("m", 0, 4), ("m", 3, 4), ("mc", 0, 1),
-    ("mc", 0, 2), ("mc", 1, 2), ("mo",),
+    ("disp",), ("pool", 1), ("pool", 3), ("pool", 2), ("m", 1, 0), ("m", 3, 0), ("pool", 0),
+    ("first",), ("m", 2, 0), ("m", 0, 0), ("m", 1, 1), ("m", 3, 1), ("m", 2, 1), ("m", 0, 1),
+    ("take",), ("got", 0), ("t", 0, 0), ("got", 2), ("t", 1, 0), ("t", 4, 0), ("t", 5, 0),
+    ("got", 1), ("t", 2, 0), ("t", 3, 0), ("got", 3), ("t", 7, 0), ("t", 1, 1), ("t", 0, 1),
+    ("t", 6, 0), ("t", 5, 1), ("t", 3, 1), ("t", 2, 1), ("t", 4, 1), ("t", 1, 2), ("t", 0, 2),
+    ("tc", 1, 0), ("t", 6, 1), ("t", 5, 2), ("t", 7, 1), ("t", 3, 2), ("tc", 2, 0), ("t", 2, 2),
+    ("t", 4, 2), ("t", 0, 3), ("t", 1, 3), ("t", 6, 2), ("tc", 0, 0), ("t", 7, 2), ("t", 3, 3),
+    ("t", 2, 3), ("tc", 0, 1), ("t", 5, 3), ("t", 4, 3), ("t", 1, 4), ("t", 0, 4), ("m", 1, 2),
+    ("t", 6, 3), ("t", 7, 3), ("tc", 0, 2), ("act", 0), ("tc", 3, 0), ("h", 1, 0), ("t", 3, 4),
+    ("h", 0, 0), ("t", 2, 4), ("tc", 1, 1), ("m", 2, 2), ("t", 5, 4), ("t", 4, 4), ("tc", 3, 1),
+    ("tc", 2, 1), ("m", 3, 2), ("tc", 1, 2), ("act", 1), ("h", 2, 0), ("tc", 2, 2), ("act", 2),
+    ("h", 4, 0), ("t", 6, 4), ("t", 7, 4), ("h", 5, 0), ("h", 3, 0), ("h", 1, 1), ("h", 0, 1),
+    ("tc", 3, 2), ("act", 3), ("h", 7, 0), ("h", 6, 0), ("h", 2, 1), ("h", 4, 1), ("mc", 0, 0),
+    ("h", 5, 1), ("h", 3, 1), ("h", 1, 2), ("h", 0, 2), ("mc", 1, 0), ("h", 7, 1), ("h", 6, 1),
+    ("h", 2, 2), ("h", 4, 2), ("h", 5, 2), ("hc", 1, 0), ("hc", 2, 0), ("h", 3, 2), ("h", 1, 3),
+    ("h", 0, 3), ("h", 7, 2), ("hc", 3, 0), ("h", 6, 2), ("m", 0, 2), ("h", 4, 3), ("h", 2, 3),
+    ("hc", 0, 0), ("h", 5, 3), ("h", 3, 3), ("h", 1, 4), ("hc", 0, 1), ("m", 3, 3), ("m", 2, 3),
+    ("h", 0, 4), ("h", 7, 3), ("h", 6, 3), ("hc", 1, 1), ("m", 1, 3), ("hc", 0, 2), ("ret", 0),
+    ("h", 4, 4), ("h", 5, 4), ("m", 0, 3), ("hc", 2, 1), ("h", 3, 4), ("h", 2, 4), ("hc", 2, 2),
+    ("ret", 2), ("h", 7, 4), ("h", 6, 4), ("hc", 1, 2), ("ret", 1), ("mc", 0, 1), ("m", 1, 4),
+    ("hc", 3, 1), ("mc", 1, 1), ("hc", 3, 2), ("ret", 3), ("m", 0, 4), ("m", 3, 4), ("m", 2, 4),
+    ("mc", 1, 2), ("mc", 0, 2), ("mo",),
 )
 
 
@@ -525,7 +524,7 @@
         bf16, f32 = jnp.bfloat16, jnp.float32
 
         sources = SOURCES if ep_size == sum(SOURCES) else (ep_size // len(SOURCES),) * len(SOURCES)
-        chunks = len(sources)
+        chunks = len(sources) * HALVES
 
         def stream_sems(groups):
             return [dma, dma((2 * groups * (ny - 1),)), dma, dma((groups, len(PARTS)))]

time: 73.4 us -> 70.8 us (0.965)
  Pallas kernels: 70.7 us -> 68.7 us
    pallas_call x1, Pallas kernels: 70.7 us -> 68.7 us  [shards(): call(*(pltpu.with_memory_space_constraint(a, pltpu.HBM) for a in operands))]
where the time goes in v4:
time: 70.8 us; the launch traced here: 70.7 us
  Pallas kernels  68.7 us (97%)
  local copies, waits for them, and re-layouts  1.33 us (2%)
    pallas_call x1, Pallas kernels, shards(): call(*(pltpu.with_memory_space_constraint(a, pltpu.HBM) for a in operands))  68.7 us

profile of v4, /device:TPU:1, one launch (start us, length us, event | category | flops | bytes accessed | tf_op | source)
XLA Modules:
  0.0 70.7 jit_solution(14440582510048645376)
XLA Ops:
  0.6 68.7 %mixer_and_experts.1 = (bf16[512,256]{1,0:T(8,128)(2,1)S(1)}, bf16[128,256]{1,0:T(8,128)(2,1)S(1)}) custom-call(bf16[512,128]{1,0:T(8,128)(2,1)} %mix_hbm.1, bf16[128,256]{1,0:T(8,128)(2,1)} %x_hbm.1, s32[2,128]{1,0:T(2,128)} %bitcast.10, f32[2,128]{1,0:T(2,128)} %bitcast.11, f32[1,4096]{1,0:T(1,128)} %bitcast.9, bf16[2048,256]{1,0:T(8,128)(2,1)} %mix_w.1, ...), custom_call_target="tpu_custom_call" | custom-call | flops 2147483648 | bytes 8388608 | tf_op jit(solution)/shard_map/mixer_and_experts/pallas_call | solution.py:596
  69.4 0.7 copy.13
  70.1 0.6 copy.14

commit v5 on v4

--- a/solution.py
+++ b/solution.py
@@ -172,7 +172,7 @@
 
     lax.fori_loop(1, ep_size, greet, 0)
 
-    for copy in in_copies:
+    for copy in in_copies[:2]:
         copy.wait()
 
     expert_rows = lax.broadcasted_iota(jnp.int32, (ep_size, tokens), 0)
@@ -199,16 +199,6 @@
     outgoing[...] = jnp.dot(
         picks.astype(jnp.bfloat16), x_in[...], preferred_element_type=jnp.float32
     ).astype(jnp.bfloat16)
-    total_share = share_in[0:1, :] + share_in[1:2, :]
-    row_id = lax.broadcasted_iota(jnp.int32, (tokens, tokens), 0)
-    packed = jnp.zeros((tokens, tokens), jnp.float32)
-    packed = jnp.where(row_id == 0, targets[0].astype(jnp.float32), packed)
-    packed = jnp.where(row_id == 1, targets[1].astype(jnp.float32), packed)
-    packed = jnp.where(row_id == 2, share_in[0:1, :] / total_share, packed)
-    packed = jnp.where(row_id == 3, share_in[1:2, :] / total_share, packed)
-    columns[...] = packed.T
-
-    ext[pl.ds(REACH, length), :] = mix_in[...].astype(jnp.float32)
     group = (tp * chans) // group_size
     window = jnp.where(group == 0, 2, jnp.where(group == 1, 4, jnp.where(group == 2, 8, 16)))
 
@@ -243,6 +233,7 @@
         device_id=(lax.rem(ep + 1, ep_size), tp),
         device_id_type=MESH,
     )
+    in_copies[3].wait()
     halo_copy.start()
 
     my_set = 0
@@ -262,6 +253,19 @@
                     device_id_type=MESH,
                 ).start()
 
+    def prepare():
+        for i in (2, 4):
+            in_copies[i].wait()
+        ext[pl.ds(REACH, length), :] = mix_in[...].astype(jnp.float32)
+        total_share = share_in[0:1, :] + share_in[1:2, :]
+        row_id = lax.broadcasted_iota(jnp.int32, (tokens, tokens), 0)
+        packed = jnp.zeros((tokens, tokens), jnp.float32)
+        packed = jnp.where(row_id == 0, targets[0].astype(jnp.float32), packed)
+        packed = jnp.where(row_id == 1, targets[1].astype(jnp.float32), packed)
+        packed = jnp.where(row_id == 2, share_in[0:1, :] / total_share, packed)
+        packed = jnp.where(row_id == 3, share_in[1:2, :] / total_share, packed)
+        columns[...] = packed.T
+
     def limit(piece, way):
         return half if (piece % 2 == 0) == (way == 0) else half - 1
 
@@ -306,7 +310,7 @@
                     ring_send(stream, piece, way, y, 0)
             mate_copy(stream, piece, y, 0)
             return
-        for way in range(2):
+        for way in (piece % 2, 1 - piece % 2):
             if hop > limit(piece, way):
                 continue
             origin = origin_of(way, hop)
@@ -443,6 +447,7 @@
             move(streams[kind], entry[1], entry[2])
         elif kind == "disp":
             dispatch()
+            prepare()
         elif kind == "take":
             find_takes()
         elif kind == "pool":

time: 70.8 us -> 70.7 us (level)
  no operation moved by 1% of the time
where the time goes in v5:
time: 70.7 us; the launch traced here: 70.6 us
  Pallas kernels  68.6 us (97%)
  local copies, waits for them, and re-layouts  1.33 us (2%)
    pallas_call x1, Pallas kernels, shards(): call(*(pltpu.with_memory_space_constraint(a, pltpu.HBM) for a in operands))  68.6 us

profile of v5, /device:TPU:1, one launch (start us, length us, event | category | flops | bytes accessed | tf_op | source)
XLA Modules:
  0.0 70.6 jit_solution(17765120044720312362)
XLA Ops:
  0.6 68.6 %mixer_and_experts.1 = (bf16[512,256]{1,0:T(8,128)(2,1)S(1)}, bf16[128,256]{1,0:T(8,128)(2,1)S(1)}) custom-call(bf16[512,128]{1,0:T(8,128)(2,1)} %mix_hbm.1, bf16[128,256]{1,0:T(8,128)(2,1)} %x_hbm.1, s32[2,128]{1,0:T(2,128)} %bitcast.10, f32[2,128]{1,0:T(2,128)} %bitcast.11, f32[1,4096]{1,0:T(1,128)} %bitcast.9, bf16[2048,256]{1,0:T(8,128)(2,1)} %mix_w.1, ...), custom_call_target="tpu_custom_call" | custom-call | flops 2147483648 | bytes 8388608 | tf_op jit(solution)/shard_map/mixer_and_experts/pallas_call | solution.py:601
  69.2 0.7 copy.13
  69.9 0.6 copy.14
